TPU v7x, 32 devices: a whole 2x2x4 slice. The times are simulated.
32 devices in a mesh: grp: 2 (over y), sp: 4 (over z), tp: 4 (over x, core).
Axes of the slice: x: 2, y: 2, z: 4, core: 2. Of those that a mesh axis runs over, the one named last changes fastest.
Arguments:
- latent: bfloat16 [2048, 2048], P(('grp', 'sp', 'tp')), parts along dimension 0, may hold values from -6 to 6
- cond: bfloat16 [4096], P(('grp', 'sp')), parts along dimension 0, may hold values from -6 to 6
- context: bfloat16 [512, 2048], P(('grp', 'sp')), parts along dimension 0, may hold values from -6 to 6
- context_cond: bfloat16 [2048], P('sp'), may hold values from -6 to 6
- norm_gain: bfloat16 [2048], replicated, may hold values from 0.099609375 to 1.8984375
- mod_shift: bfloat16 [2048, 2048], P('sp', 'tp'), may hold values from -0.125 to 0.125
- mod_scale: bfloat16 [2048, 2048], P('sp', 'tp'), may hold values from -0.125 to 0.125
- mod_gate: bfloat16 [2048, 2048], P('sp', 'tp'), may hold values from -0.125 to 0.125
- w_query: bfloat16 [2048, 2048], P(None, 'tp'), may hold values from -0.125 to 0.125
- w_key: bfloat16 [2048, 2048], P(None, 'tp'), may hold values from -0.125 to 0.125
- w_value: bfloat16 [2048, 4096], P(None, 'tp'), may hold values from -0.125 to 0.125
- w_gate: bfloat16 [2048, 4096], P(None, 'tp'), may hold values from -0.125 to 0.125
- w_out: bfloat16 [4096, 2048], P('tp'), may hold values from -0.09375 to 0.09375
- decay_rate: float32 [2, 8], P(None, 'tp'), may hold values from 0.00015625 to 0.034
- context_gain: float32 [8], P('tp'), may hold values from 3 to 10
Outputs:
- mixed: bfloat16 [2048, 2048], P(('grp', 'sp', 'tp')), parts along dimension 0
There are 2 independent parts, one for each index of `grp`. A program takes and returns all parts, laid end to end along the dimension named above; an argument that names none is the same for every part. Nothing has to cross between parts.
All inputs are finite; a program needn't handle non-finite values.
Results may differ from a plain program's by a relative error of at most 0.009.
Values may be sent and summed in bfloat16 or wider, within the bound.
A program may use at most 128 MiB of HBM per device.

v0:
```python
import functools
import math

import jax
import jax.numpy as jnp
from jax import lax
from jax.experimental import pallas as pl
from jax.experimental.pallas import tpu as pltpu
from jax.sharding import PartitionSpec as P

DK = 256
GRID_W = 128
TILE = 256
CHUNK = 64
LAG = 2
norm_eps = 1e-06
rope_base = 10000.0
MESH = pl.DeviceIdType.MESH
F32, BF16 = jnp.float32, jnp.bfloat16


def dot(a, b):
    return jnp.dot(a, b, preferred_element_type=F32)


def dot_tn(a, b):
    return lax.dot_general(a, b, (((0,), (0,)), ((), ())), preferred_element_type=F32)


def dot_nt(a, b):
    return lax.dot_general(a, b, (((1,), (1,)), ((), ())), preferred_element_type=F32)


def remote(src, dst, send, recv, where):
    return pltpu.make_async_remote_copy(
        src_ref=src, dst_ref=dst, send_sem=send, recv_sem=recv, device_id=where, device_id_type=MESH
    )


def rows_of(start, size):
    return pl.ds(pl.multiple_of(start, size), size)


def kernel(
    S,
    T,
    latent,
    cond,
    context,
    norm_gain,
    mod_shift,
    mod_scale,
    mod_gate,
    w_query,
    w_key,
    w_value,
    w_gate,
    w_out,
    decay,
    gain,
    out,
    x_all,
    c_all,
    h_ref,
    hc_ref,
    m_shift,
    m_scale,
    m_gate,
    vq,
    vk,
    vv,
    vg,
    vo,
    m_send,
    m_sp,
    m_tp,
    mod,
    cos_t,
    sin_t,
    q_ref,
    k_ref,
    v_ref,
    ck_ref,
    cv_ref,
    g_ref,
    ret_ref,
    gated,
    loc,
    st_in,
    st_out,
    part,
    p1,
    p2,
    xs,
    xr,
    load_sem,
    lat_send,
    lat_recv,
    ctx_send,
    ctx_fsend,
    ctx_recv,
    msp_send,
    msp_recv,
    mtp_send,
    mtp_recv,
    st_send,
    st_recv,
    p1_send,
    p1_recv,
    p2_send,
    p2_recv,
    x_send,
    x_recv,
):
    sp, tp = lax.axis_index("sp"), lax.axis_index("tp")
    R, D = latent.shape
    Cr = context.shape[0]
    half = Cr // 2
    CT = Cr * S
    span = R * T
    nh = w_query.shape[1] // DK
    DV = w_value.shape[1] // nh
    Mc = mod_shift.shape[1]
    X = T // 2
    chip, core = tp // 2, lax.rem(tp, 2)
    partner = tp + 1 - 2 * core
    is_end = jnp.logical_or(sp == 0, sp == S - 1)
    NC = part.shape[0]
    W = D // NC

    loads = [
        pltpu.make_async_copy(src, dst, load_sem.at[i])
        for i, (src, dst) in enumerate(
            [
                (mod_shift, m_shift),
                (mod_scale, m_scale),
                (mod_gate, m_gate),
                (latent, x_all.at[rows_of(tp * R, R)]),
                (context, c_all.at[rows_of(sp * Cr, Cr)]),
                (w_key, vk),
                (w_value, vv),
                (w_query, vq),
                (w_gate, vg),
                (w_out, vo),
            ]
        )
    ]
    for copy in loads:
        copy.start()

    barrier = pltpu.get_barrier_semaphore()
    for k in range(1, S):
        pl.semaphore_signal(
            barrier, inc=1, device_id={"sp": lax.rem(sp + k, S)}, device_id_type=MESH
        )
    for k in range(1, T):
        pl.semaphore_signal(
            barrier, inc=1, device_id={"tp": lax.rem(tp + k, T)}, device_id_type=MESH
        )
    pl.semaphore_wait(barrier, S + T - 2)

    def lat_copy(src, owner, to, which):
        place = rows_of(owner * R, R)
        return remote(
            latent if src is None else x_all.at[place],
            x_all.at[place],
            lat_send.at[which, to if which == 0 else owner],
            lat_recv.at[owner],
            {"tp": to},
        )

    others = [lax.rem(chip + k, X) for k in range(1, X)]
    direct = [lat_copy(None, tp, 2 * o + core, 0) for o in others] + [
        lat_copy(None, tp, partner, 0)
    ]
    for copy in direct:
        copy.start()

    def ctx_copy(src_ref, owner, part_core, send, recv, where):
        place = rows_of(owner * Cr + part_core * half, half)
        src = context.at[rows_of(part_core * half, half)] if src_ref is None else c_all.at[place]
        return remote(src, c_all.at[place], send, recv, where)

    ends = (0, S - 1)

    def ctx_out(e):
        return ctx_copy(None, sp, core, ctx_send.at[e], ctx_recv.at[0, sp], {"sp": ends[e]})

    for e in range(2):

        @pl.when(sp != ends[e])
        def _():
            ctx_out(e).start()

    for copy in loads[:3]:
        copy.wait()
    rows = cond[...]
    m_send[...] = jnp.zeros_like(m_send)
    m_send[0:2] = dot(rows, m_shift[...])[0:2]
    m_send[2:4] = dot(rows, m_scale[...])[0:2]
    m_send[4:5] = dot(rows, m_gate[...])[0:1]

    def sp_copy(owner, to):
        return remote(m_send, m_sp.at[owner], msp_send.at[to], msp_recv.at[owner], {"sp": to})

    sp_peers = [lax.rem(sp + k, S) for k in range(1, S)]
    tp_peers = [lax.rem(tp + k, T) for k in range(1, T)]
    for p in sp_peers:
        sp_copy(sp, p).start()

    F = DK // 4
    pos = (lax.broadcasted_iota(jnp.int32, (span, 2 * F), 0) + sp * span).astype(F32)
    lane = lax.broadcasted_iota(jnp.int32, (span, 2 * F), 1)
    grid_row = jnp.floor(pos * (1.0 / GRID_W))
    grid_col = pos - grid_row * GRID_W
    freq = jnp.where(lane < F, lane, lane - F).astype(F32)
    angle = jnp.where(lane < F, grid_row, grid_col) * jnp.exp(
        freq * (-math.log(rope_base) / F)
    )
    cos_t[...] = jnp.cos(angle)
    sin_t[...] = jnp.sin(angle)

    total = m_send[...]
    for p in sp_peers:
        sp_copy(p, p).wait_recv()
        total = total + m_sp[p]
    m_tp[tp] = total

    def tp_copy(owner, to):
        return remote(
            m_tp.at[owner], m_tp.at[owner], mtp_send.at[to], mtp_recv.at[owner], {"tp": to}
        )

    for p in tp_peers:
        tp_copy(tp, p).start()

    forwards = []
    for o in others:
        owner = 2 * o + core
        lat_copy(None, owner, owner, 0).wait_recv()
        copy = lat_copy(1, owner, partner, 1)
        copy.start()
        forwards.append(copy)
    loads[3].wait()

    for p in tp_peers:
        tp_copy(p, p).wait_recv()
    for t in range(T):
        mod[:, t * Mc : (t + 1) * Mc] = m_tp[t]

    def modulate(src, dst, start, count, row):
        mult = norm_gain[...].astype(F32) * (1.0 + mod[2 + row : 3 + row, :])
        shift = mod[row : row + 1, :]
        size = min(32, count)

        def lap(i, _):
            place = rows_of(start + i * size, size)
            x = src[place, :].astype(F32)
            scale = lax.rsqrt(jnp.mean(x * x, axis=-1, keepdims=True) + norm_eps)
            dst[place, :] = (x * scale * mult + shift).astype(BF16)
            return 0

        lax.fori_loop(0, count // size, lap, 0)

    modulate(x_all, h_ref, tp * R, R, 0)
    for o in others:
        modulate(x_all, h_ref, (2 * o + core) * R, R, 0)
    lat_copy(None, partner, partner, 0).wait_recv()
    modulate(x_all, h_ref, partner * R, R, 0)
    for o in others:
        owner = 2 * o + 1 - core
        lat_copy(None, owner, owner, 0).wait_recv()
        modulate(x_all, h_ref, owner * R, R, 0)

    scale_k = DK**-0.5

    def rotated(x):
        u, w = x[:, : DK // 2], x[:, DK // 2 :]
        c, s = cos_t[...], sin_t[...]
        return jnp.concatenate([u * c - w * s, w * c + u * s], axis=1).astype(BF16)

    def cols(j, size):
        return pl.ds(pl.multiple_of(j * size, size), size)

    loads[4].wait()

    @pl.when(is_end)
    def _():
        for p in sp_peers:
            ctx_copy(None, p, core, ctx_send.at[0], ctx_recv.at[0, p], {"sp": p}).wait_recv()
            ctx_copy(1, p, core, ctx_fsend.at[p], ctx_recv.at[1, p], {"tp": partner}).start()

    loads[5].wait()

    def key_tile(h, _):
        k_ref[h] = rotated(dot(h_ref[...], vk[:, cols(h, DK)]) * scale_k)
        return 0

    lax.fori_loop(0, nh, key_tile, 0)
    loads[6].wait()

    def value_tile(j, _):
        v_ref[:, cols(j, TILE)] = dot(h_ref[...], vv[:, cols(j, TILE)]).astype(BF16)
        return 0

    lax.fori_loop(0, nh * DV // TILE, value_tile, 0)

    def local_states(h, _):
        k = k_ref[h].astype(F32)
        v = v_ref[:, cols(h, DV)]
        place = lax.broadcasted_iota(jnp.int32, (span, DK), 0).astype(F32)
        fk = (k * jnp.exp(-decay[0, h] * (span - 1.0 - place))).astype(BF16)
        bk = (k * jnp.exp(-decay[1, h] * place)).astype(BF16)
        loc[0, cols(h, DK), :] = dot_tn(fk, v)
        loc[1, cols(h, DK), :] = dot_tn(bk, v)
        return 0

    lax.fori_loop(0, nh, local_states, 0)

    @pl.when(is_end)
    def _():
        for p in sp_peers:
            ctx_copy(
                1, p, 1 - core, ctx_fsend.at[p], ctx_recv.at[1, p], {"tp": partner}
            ).wait_recv()
        modulate(c_all, hc_ref, 0, CT, 1)
        M = min(CT, TILE)
        at_start = sp == 0
        side = jnp.where(at_start, 0, 1)

        def ctx_rows(r, _):
            place = rows_of(r * M, M)

            def ctx_key(h, _):
                ck_ref[h, place, :] = (dot(hc_ref[place, :], vk[:, cols(h, DK)]) * scale_k).astype(
                    BF16
                )
                return 0

            lax.fori_loop(0, nh, ctx_key, 0)

            def ctx_value(j, _):
                cv_ref[place, cols(j, TILE)] = dot(hc_ref[place, :], vv[:, cols(j, TILE)]).astype(
                    BF16
                )
                return 0

            lax.fori_loop(0, nh * DV // TILE, ctx_value, 0)
            return 0

        lax.fori_loop(0, CT // M, ctx_rows, 0)

        def ctx_state(h, _):
            place = lax.broadcasted_iota(jnp.int32, (CT, DK), 0).astype(F32)
            rate = jnp.where(at_start, decay[0, h], decay[1, h])
            away = jnp.where(at_start, CT - 1.0 - place, place)
            keys = (ck_ref[h].astype(F32) * jnp.exp(-rate * away)).astype(BF16)
            state = dot_tn(keys, cv_ref[:, cols(h, DV)]) * gain[h]
            st_in[side, cols(h, DK), :] = state.astype(BF16)
            return 0

        lax.fori_loop(0, nh, ctx_state, 0)

    n = nh * DK // CHUNK
    hop = (sp, S - 1 - sp)
    after = (sp + 1, sp - 1)
    before = (sp - 1, sp + 1)
    per_head = DK // CHUNK

    def st_copy(d, c, to):
        place = rows_of(c * CHUNK, CHUNK)
        return remote(
            st_out.at[d, place],
            st_in.at[d, place],
            st_send.at[d, c],
            st_recv.at[d, c],
            {"sp": to},
        )

    def relay(d, c):
        @pl.when(hop[d] > 0)
        def _():
            st_copy(d, c, before[d]).wait_recv()

        @pl.when(hop[d] < S - 1)
        def _():
            place = rows_of(c * CHUNK, CHUNK)
            fade = jnp.exp(jnp.full((1, DV), -decay[d, c // per_head] * span, F32))
            st_out[d, place, :] = (st_in[d, place, :].astype(F32) * fade + loc[d, place, :]).astype(
                BF16
            )
            st_copy(d, c, after[d]).start()

    ng = nh * DV // TILE
    loads[7].wait()
    loads[8].wait()

    def lap(i, _):
        for d in range(2):
            c = i - LAG * hop[d]

            @pl.when(jnp.logical_and(c >= 0, c < n))
            def _():
                relay(d, c)

        @pl.when(i < nh)
        def _():
            q_ref[i] = rotated(dot(h_ref[...], vq[:, cols(i, DK)]))

        @pl.when(jnp.logical_and(i >= nh, i < nh + ng))
        def _():
            pre = dot(h_ref[...], vg[:, cols(i - nh, TILE)])
            g_ref[:, cols(i - nh, TILE)] = pre / (1.0 + jnp.exp(-pre))

        @pl.when(jnp.logical_and(i >= nh + ng, i < 2 * nh + ng))
        def _():
            h = i - nh - ng
            row = lax.broadcasted_iota(jnp.int32, (span, span), 0)
            col = lax.broadcasted_iota(jnp.int32, (span, span), 1)
            gap = (row - col).astype(F32)
            mask = jnp.where(gap >= 0, jnp.exp(-decay[0, h] * jnp.maximum(gap, 0.0)), 0.0)
            mask += jnp.where(gap <= 0, jnp.exp(-decay[1, h] * jnp.maximum(-gap, 0.0)), 0.0)
            weights = (dot_nt(q_ref[h], k_ref[h]) * mask).astype(BF16)
            ret_ref[h] = dot(weights, v_ref[:, cols(h, DV)])

        return 0

    lax.fori_loop(0, max(n + LAG * (S - 1), 2 * nh + ng), lap, 0)

    def finish(h, _):
        place = lax.broadcasted_iota(jnp.int32, (span, DV), 0).astype(F32)
        q = q_ref[h]
        ret = (
            ret_ref[h]
            + dot(q, st_in[0, cols(h, DK), :]) * jnp.exp(-decay[0, h] * (place + 1.0))
            + dot(q, st_in[1, cols(h, DK), :]) * jnp.exp(-decay[1, h] * (span - place))
        )
        ret = ret - jnp.mean(ret, axis=-1, keepdims=True)
        ret = ret * lax.rsqrt(jnp.mean(ret * ret, axis=-1, keepdims=True) + norm_eps)
        gated[:, cols(h, DV)] = (g_ref[:, cols(h, DV)] * ret).astype(BF16)
        return 0

    lax.fori_loop(0, nh, finish, 0)
    loads[9].wait()

    def p1_copy(c, o):
        return remote(
            part.at[c, 2 * o + 1 - core],
            p1.at[c, o],
            p1_send.at[c, o],
            p1_recv.at[c, o],
            {"tp": partner},
        )

    def p2_copy(c):
        return remote(
            part.at[c, partner], p2.at[c], p2_send.at[c], p2_recv.at[c], {"tp": partner}
        )

    def x_copy(c, owner, o):
        return remote(
            xs.at[c, o], xr.at[c, owner], x_send.at[c, o], x_recv.at[c, owner], {"tp": 2 * o + core}
        )

    def across(c):
        for o in others:
            p1_copy(c, o).wait_recv()
            mine = part[c, 2 * o + core].astype(F32)
            xs[c, o] = (mine + p1[c, o].astype(F32)).astype(BF16)
            x_copy(c, chip, o).start()

    def project(c, _):
        product = dot(gated[...], vo[:, cols(c, W)]).astype(BF16)
        for t in range(T):
            part[c, t] = product[t * R : (t + 1) * R, :]
        for o in others:
            p1_copy(c, o).start()
        p2_copy(c).start()

        @pl.when(c > 0)
        def _():
            across(c - 1)

        return 0

    lax.fori_loop(0, NC, project, 0)
    across(NC - 1)

    def final(c, _):
        p2_copy(c).wait_recv()
        total = part[c, tp].astype(F32) + p2[c].astype(F32)
        for o in others:
            x_copy(c, o, o).wait_recv()
            total = total + xr[c, o].astype(F32)
        mine = x_all[rows_of(tp * R, R), cols(c, W)].astype(F32)
        out[:, cols(c, W)] = (mine + mod[4:5, cols(c, W)] * total).astype(BF16)
        return 0

    lax.fori_loop(0, NC, final, 0)

    for copy in direct + forwards:
        copy.wait_send()
    for e in range(2):

        @pl.when(sp != ends[e])
        def _():
            ctx_out(e).wait_send()

    @pl.when(is_end)
    def _():
        for p in sp_peers:
            ctx_copy(1, p, core, ctx_fsend.at[p], ctx_recv.at[1, p], {"tp": partner}).wait_send()

    for p in sp_peers:
        sp_copy(sp, p).wait_send()
    for p in tp_peers:
        tp_copy(tp, p).wait_send()

    def sent(c, _):
        for d in range(2):

            @pl.when(hop[d] < S - 1)
            def _():
                st_copy(d, c, after[d]).wait_send()

        return 0

    lax.fori_loop(0, n, sent, 0)

    def sent_out(c, _):
        for o in others:
            p1_copy(c, o).wait_send()
            x_copy(c, chip, o).wait_send()
        p2_copy(c).wait_send()
        return 0

    lax.fori_loop(0, NC, sent_out, 0)


def body(
    S,
    T,
    latent,
    cond,
    context,
    context_cond,
    norm_gain,
    mod_shift,
    mod_scale,
    mod_gate,
    w_query,
    w_key,
    w_value,
    w_gate,
    w_out,
    decay_rate,
    context_gain,
):
    R, D = latent.shape
    Cr = context.shape[0]
    span, CT = R * T, Cr * S
    nh = w_query.shape[1] // DK
    DV = w_value.shape[1] // nh
    Mr, Mc = mod_shift.shape
    X = T // 2
    NC = 4
    W = D // NC
    n = nh * DK // CHUNK
    rows = jnp.concatenate(
        [cond[None], context_cond[None], jnp.zeros((14, Mr), cond.dtype)]
    ).astype(F32)
    rows = jax.nn.silu(rows).astype(BF16)
    VMEM = pl.BlockSpec(memory_space=pltpu.VMEM)
    ANY = pl.BlockSpec(memory_space=pl.ANY)
    SMEM = pl.BlockSpec(memory_space=pltpu.SMEM)
    v = pltpu.VMEM
    DMA = pltpu.SemaphoreType.DMA
    return pl.pallas_call(
        functools.partial(kernel, S, T),
        out_shape=jax.ShapeDtypeStruct((R, D), BF16),
        in_specs=[ANY, VMEM, ANY, VMEM] + [ANY] * 8 + [SMEM, SMEM],
        out_specs=VMEM,
        scratch_shapes=[
            v((span, D), BF16),
            v((CT, D), BF16),
            v((span, D), BF16),
            v((CT, D), BF16),
            v((Mr, Mc), BF16),
            v((Mr, Mc), BF16),
            v((Mr, Mc), BF16),
            v(w_query.shape, BF16),
            v(w_key.shape, BF16),
            v(w_value.shape, BF16),
            v(w_gate.shape, BF16),
            v(w_out.shape, BF16),
            v((8, Mc), F32),
            v((S, 8, Mc), F32),
            v((T, 8, Mc), F32),
            v((8, D), F32),
            v((span, DK // 2), F32),
            v((span, DK // 2), F32),
            v((nh, span, DK), BF16),
            v((nh, span, DK), BF16),
            v((span, nh * DV), BF16),
            v((nh, CT, DK), BF16),
            v((CT, nh * DV), BF16),
            v((span, nh * DV), F32),
            v((nh, span, DV), F32),
            v((span, nh * DV), BF16),
            v((2, nh * DK, DV), F32),
            v((2, nh * DK, DV), BF16),
            v((2, nh * DK, DV), BF16),
            v((NC, T, R, W), BF16),
            v((NC, X, R, W), BF16),
            v((NC, R, W), BF16),
            v((NC, X, R, W), BF16),
            v((NC, X, R, W), BF16),
            DMA((10,)),
            DMA((2, T)),
            DMA((T,)),
            DMA((2,)),
            DMA((S,)),
            DMA((2, S)),
            DMA((S,)),
            DMA((S,)),
            DMA((T,)),
            DMA((T,)),
            DMA((2, n)),
            DMA((2, n)),
            DMA((NC, X)),
            DMA((NC, X)),
            DMA((NC,)),
            DMA((NC,)),
            DMA((NC, X)),
            DMA((NC, X)),
        ],
        compiler_params=pltpu.CompilerParams(
            collective_id=0, has_side_effects=True, vmem_limit_bytes=60 * 1024 * 1024
        ),
    )(
        latent,
        rows,
        context,
        norm_gain[None],
        mod_shift,
        mod_scale,
        mod_gate,
        w_query,
        w_key,
        w_value,
        w_gate,
        w_out,
        decay_rate,
        context_gain,
    )


def solution(mesh):
    return jax.shard_map(
        functools.partial(body, mesh.shape["sp"], mesh.shape["tp"]),
        mesh=mesh,
        in_specs=(
            P(("grp", "sp", "tp"), None),
            P(("grp", "sp")),
            P(("grp", "sp"), None),
            P("sp"),
            P(),
            P("sp", "tp"),
            P("sp", "tp"),
            P("sp", "tp"),
            P(None, "tp"),
            P(None, "tp"),
            P(None, "tp"),
            P(None, "tp"),
            P("tp", None),
            P(None, "tp"),
            P("tp"),
        ),
        out_specs=P(("grp", "sp", "tp"), None),
        check_vma=False,
    )
```

profile of v0, /device:TPU:0, one launch (start us, length us, event | category | flops | bytes accessed | tf_op | source)
XLA Modules:
  0.0 67.9 jit_solution(10801270178127905132)
XLA Ops:
  0.0 0.1 pad.2.clone
  0.1 0.7 %broadcast_in_dim.12 = bf16[1,512]{1,0:T(2,128)(2,1)S(1)} reshape(bf16[512]{0:T(512)(128)(2,1)} %param.16) | data formatting | bytes 2048 | tf_op jit(solution)/shard_map/broadcast_in_dim | solution.py:570
  0.8 0.7 %broadcast_in_dim.13 = bf16[1,512]{1,0:T(2,128)(2,1)S(1)} reshape(bf16[512]{0:T(512)(128)(2,1)} %param.18) | data formatting | bytes 2048 | tf_op jit(solution)/shard_map/broadcast_in_dim | solution.py:570
  1.4 1.3 %broadcast_in_dim.15.norm_gain = bf16[1,2048]{1,0:T(2,128)(2,1)} reshape(bf16[2048]{0:T(1024)(128)(2,1)} %param.19) | data formatting | bytes 8192 | tf_op jit(solution)/shard_map/broadcast_in_dim | solution.py:644
  2.7 0.7 %fusion.3.cond = bf16[16,512]{1,0:T(8,128)(2,1)} fusion(bf16[1,512]{1,0:T(2,128)(2,1)S(1)} %broadcast_in_dim.13, bf16[1,512]{1,0:T(2,128)(2,1)S(1)} %broadcast_in_dim.12, bf16[16]{0:T(256)(128)(2,1)S(1)} %pad.2.clone), kind=kLoop, calls=%fused_computation.5 | loop fusion | flops 90112 | bytes 18464 | tf_op jit(solution)/shard_map/convert_element_type | solution.py:572
  3.4 62.8 %shard_map.145 = bf16[64,2048]{1,0:T(8,128)(2,1)} custom-call(bf16[64,2048]{1,0:T(8,128)(2,1)} %latent.1, bf16[16,512]{1,0:T(8,128)(2,1)} %fusion.3.cond, bf16[64,2048]{1,0:T(8,128)(2,1)} %context.1, bf16[1,2048]{1,0:T(2,128)(2,1)} %broadcast_in_dim.15.norm_gain, bf16[512,512]{1,0:T(8,128)(2,1)} %mod_shift.1, bf16[512,512]{1,0:T(8,128)(2,1)} %mod_scale.1, ...), custom_call_target="tpu_custom_call" | custom-call | tf_op jit(solution)/shard_map/pallas_call | solution.py:578
  66.3 1.7 %copy.17 = bf16[64,2048]{1,0:T(8,128)(2,1)} copy(bf16[64,2048]{1,0:T(8,128)(2,1)} %shard_map.145) | data formatting | bytes 524288
  (1 shorter events, 0.0 us)
where the time goes:
time: 68.2 us; the launch traced here: 67.9 us
  Pallas kernels  62.8 us (92%)
  local copies, waits for them, and re-layouts  4.4 us (6%)
  other arithmetic  0.69 us (1%)
    pallas_call x1, Pallas kernels, body(): pl.pallas_call(functools.partial(kernel, S, T), out_shape=jax.ShapeDtypeS...  62.8 us
    unnamed x1, local copies, waits for them, and re-layouts  1.67 us

commit v1 on v0

v1 whole, which is shorter than its diff:
```python
import functools
import math
from types import SimpleNamespace

import jax
import jax.numpy as jnp
from jax import lax
from jax.experimental import pallas as pl
from jax.experimental.pallas import tpu as pltpu
from jax.sharding import PartitionSpec as P

DK = 256
GRID_W = 128
TILE = 256
PIECE = 16
CHUNK = 32
LAG = 5
PRE = 3
NC = 4
norm_eps = 1e-06
rope_base = 10000.0
MESH = pl.DeviceIdType.MESH
F32, BF16 = jnp.float32, jnp.bfloat16


def dot(a, b):
    return jnp.dot(a, b, preferred_element_type=F32)


def dot_tn(a, b):
    return lax.dot_general(a, b, (((0,), (0,)), ((), ())), preferred_element_type=F32)


def dot_nt(a, b):
    return lax.dot_general(a, b, (((1,), (1,)), ((), ())), preferred_element_type=F32)


def remote(src, dst, send, recv, where):
    return pltpu.make_async_remote_copy(
        src_ref=src, dst_ref=dst, send_sem=send, recv_sem=recv, device_id=where, device_id_type=MESH
    )


def rows_of(start, size):
    return pl.ds(pl.multiple_of(start, size), size)


def cols(j, size):
    return pl.ds(pl.multiple_of(j * size, size), size)


def tiled(x, count):
    return jnp.concatenate([x] * count, axis=0) if count > 1 else x


def kernel(S, T, names, *refs):
    (
        latent,
        cond,
        context_cond,
        context,
        norm_gain,
        mod_shift,
        mod_scale,
        mod_gate,
        w_query,
        w_key,
        w_value,
        w_gate,
        w_out,
        decay_in,
        gain_in,
        out,
    ) = refs[:16]
    r = SimpleNamespace(**dict(zip(names, refs[16:])))

    sp, tp = lax.axis_index("sp"), lax.axis_index("tp")
    R, D = latent.shape
    Cr = context.shape[0]
    half = Cr // 2
    CT = Cr * S
    span = R * T
    nh = w_query.shape[1] // DK
    DV = w_value.shape[1] // nh
    Mr, Mc = mod_shift.shape
    G, GD = Mc // 128, D // 128
    X = T // 2
    pieces = R // PIECE
    chip, core = tp // 2, lax.rem(tp, 2)
    partner = tp + 1 - 2 * core
    is_end = jnp.logical_or(sp == 0, sp == S - 1)
    W = D // NC
    per_head = DK // CHUNK
    n = nh * per_head
    hop = (sp, S - 1 - sp)
    after = (sp + 1, sp - 1)
    before = (sp - 1, sp + 1)
    sp_peers = [lax.rem(sp + k, S) for k in range(1, S)]
    others = [lax.rem(chip + k, X) for k in range(1, X)]
    peers = [
        (lax.rem(sp + i, S), lax.rem(tp + j, T)) for i in range(S) for j in range(T) if i or j
    ]

    barrier = pltpu.get_barrier_semaphore()
    for a, b in peers:
        pl.semaphore_signal(
            barrier, inc=1, device_id={"sp": a, "tp": b}, device_id_type=MESH
        )

    own = rows_of(tp * R, R)
    pairs = [
        (cond, r.cond),
        (context_cond, r.ccond),
        (mod_shift, r.m_shift),
        (mod_scale, r.m_scale),
        (latent, r.x_all.at[own]),
        (mod_gate, r.m_gate),
        (decay_in, r.decay),
        (gain_in, r.gain),
        (norm_gain, r.ngain),
        (context, r.c_all.at[rows_of(sp * Cr, Cr)]),
        (w_key, r.vk),
        (w_value, r.vv),
        (w_query, r.vq),
        (w_gate, r.vg),
        (w_out, r.vo),
    ]
    loads = [
        pltpu.make_async_copy(src, dst, r.load_sem.at[i]) for i, (src, dst) in enumerate(pairs)
    ]
    for copy in loads:
        copy.start()

    for copy in loads[:2]:
        copy.wait()

    def silu_row(ref):
        v = ref[...].astype(F32)
        v = v / (1.0 + jnp.exp(-v))
        return jnp.concatenate([v[g : g + 1, :] for g in range(Mr // 128)], axis=1)

    rows = jnp.concatenate(
        [silu_row(r.cond), silu_row(r.ccond), jnp.zeros((14, Mr), F32)], axis=0
    ).astype(BF16)
    loads[2].wait()
    shift_part = dot(rows, r.m_shift[...])
    loads[3].wait()
    scale_part = dot(rows, r.m_scale[...])

    def lanes(x, row, g):
        return x[row : row + 1, g * 128 : (g + 1) * 128]

    for g in range(G):
        r.m1[sp, tp, g : g + 1, :] = lanes(shift_part, 0, g)
        r.m1[sp, tp, G + g : G + g + 1, :] = lanes(scale_part, 0, g)

    def m1_copy(owner, to, k):
        slot = r.m1.at[owner[0], owner[1]]
        return remote(slot, slot, r.m1_send.at[k], r.m1_recv.at[k], {"sp": to[0], "tp": to[1]})

    def m2_copy(owner, to, k):
        slot = r.m2.at[owner[0], owner[1]]
        return remote(slot, slot, r.m2_send.at[k], r.m2_recv.at[k], {"sp": to[0], "tp": to[1]})

    def lat_copy(owner, p, to, which):
        place = rows_of(owner * R + p * PIECE, PIECE)
        return remote(
            r.x_all.at[place],
            r.x_all.at[place],
            r.lat_send.at[which, to if which == 0 else owner, p],
            r.lat_recv.at[owner, p],
            {"tp": to},
        )

    def ctx_copy(owner, part_core, send, recv, where):
        place = rows_of(owner * Cr + part_core * half, half)
        return remote(r.c_all.at[place], r.c_all.at[place], send, recv, where)

    def ctx_out(to):
        return ctx_copy(sp, core, r.ctx_send.at[to], r.ctx_recv.at[0, sp], {"sp": to})

    loads[4].wait()
    pl.semaphore_wait(barrier, len(peers))

    for k, to in enumerate(peers):
        m1_copy((sp, tp), to, k).start()
    for p in range(pieces):
        for o in others:
            lat_copy(tp, p, 2 * o + core, 0).start()
    for p in range(pieces):
        lat_copy(tp, p, partner, 0).start()

    gate_wait = loads[5]
    gate_wait.wait()
    gate_part = dot(rows, r.m_gate[...])
    for g in range(G):
        r.m2[sp, tp, g : g + 1, :] = lanes(shift_part, 1, g)
        r.m2[sp, tp, G + g : G + g + 1, :] = lanes(scale_part, 1, g)
        r.m2[sp, tp, 2 * G + g : 2 * G + g + 1, :] = lanes(gate_part, 0, g)
    loads[9].wait()
    for k, to in enumerate(peers):
        m2_copy((sp, tp), to, k).start()
    for to in sp_peers:
        ctx_out(to).start()

    F = DK // 4
    pos = (lax.broadcasted_iota(jnp.int32, (span, 2 * F), 0) + sp * span).astype(F32)
    lane = lax.broadcasted_iota(jnp.int32, (span, 2 * F), 1)
    grid_row = jnp.floor(pos * (1.0 / GRID_W))
    grid_col = pos - grid_row * GRID_W
    freq = jnp.where(lane < F, lane, lane - F).astype(F32)
    angle = jnp.where(lane < F, grid_row, grid_col) * jnp.exp(freq * (-math.log(rope_base) / F))
    r.cos_t[...] = jnp.cos(angle)
    r.sin_t[...] = jnp.sin(angle)

    for copy in loads[6:9]:
        copy.wait()

    def decay_tables(h, _):
        a, b = r.decay[0, h], r.decay[1, h]
        place = lax.broadcasted_iota(jnp.int32, (span, 128), 0).astype(F32)
        r.ktab[0, h] = jnp.exp(-a * (span - 1.0 - place))
        r.ktab[1, h] = jnp.exp(-b * place)
        r.qtab[0, h] = jnp.exp(-a * (place + 1.0))
        r.qtab[1, h] = jnp.exp(-b * (span - place))
        far = lax.broadcasted_iota(jnp.int32, (CT, 128), 0).astype(F32)
        r.ctab[0, h] = jnp.exp(-a * (CT - 1.0 - far))
        r.ctab[1, h] = jnp.exp(-b * far)
        for d, rate in enumerate((a, b)):
            r.fade[d, h] = jnp.exp(jnp.full((8, DV), -rate * span, F32))
        gap = (
            lax.broadcasted_iota(jnp.int32, (span, span), 0)
            - lax.broadcasted_iota(jnp.int32, (span, span), 1)
        ).astype(F32)
        mask = jnp.where(gap >= 0, jnp.exp(-a * jnp.maximum(gap, 0.0)), 0.0)
        mask += jnp.where(gap <= 0, jnp.exp(-b * jnp.maximum(-gap, 0.0)), 0.0)
        r.mask[h] = mask
        return 0

    lax.fori_loop(0, nh, decay_tables, 0)

    def stat(src, dst, start, count):
        place = rows_of(start, count)
        x = src[place, :].astype(F32)
        inv = lax.rsqrt(jnp.mean(x * x, axis=-1, keepdims=True) + norm_eps)
        dst[place, :] = jnp.broadcast_to(inv, (count, 128))

    def apply(src, dst, inv, start, count, row):
        place = rows_of(start, count)
        scale = inv[place, :]
        for j in range(GD):
            c = slice(j * 128, (j + 1) * 128)
            mult = tiled(r.mult[row, :, c], count // 8)
            shift = tiled(r.shift[row, :, c], count // 8)
            dst[place, c] = (src[place, c].astype(F32) * scale * mult + shift).astype(BF16)

    def spread(row, source, at_shift, at_scale):
        for t in range(T):
            total = source[0, t]
            for s in range(1, S):
                total = total + source[s, t]
            r.g16[0, t * G : (t + 1) * G, :] = total[at_shift : at_shift + G]
            r.g16[1, t * G : (t + 1) * G, :] = total[at_scale : at_scale + G]
            if row:
                r.g16[2, t * G : (t + 1) * G, :] = total[2 * G : 3 * G]
        r.g16[1] = r.ngain[...].astype(F32) * (1.0 + r.g16[1])
        for j in range(GD):
            c = slice(j * 128, (j + 1) * 128)
            r.shift[row, :, c] = jnp.broadcast_to(r.g16[0, j : j + 1, :], (8, 128))
            r.mult[row, :, c] = jnp.broadcast_to(r.g16[1, j : j + 1, :], (8, 128))
            if row:
                r.gate[:, c] = jnp.broadcast_to(r.g16[2, j : j + 1, :], (8, 128))

    stat(r.x_all, r.inv, tp * R, R)
    for p in range(pieces - 1):
        for o in others:
            lat_copy(2 * o + core, p, tp, 0).wait_recv()
            lat_copy(2 * o + core, p, partner, 1).start()
    opposite = [(lax.rem(sp - i + S, S), lax.rem(tp - j + T, T)) for i in range(S) for j in range(T) if i or j]
    for k, (a, b) in enumerate(opposite):
        m1_copy((a, b), (a, b), k).wait_recv()
    spread(0, r.m1, 0, G)
    apply(r.x_all, r.h, r.inv, tp * R, R, 0)
    for o in others:
        lat_copy(2 * o + core, pieces - 1, tp, 0).wait_recv()
        lat_copy(2 * o + core, pieces - 1, partner, 1).start()
        stat(r.x_all, r.inv, (2 * o + core) * R, R)
        apply(r.x_all, r.h, r.inv, (2 * o + core) * R, R, 0)
    for p in range(pieces):
        lat_copy(partner, p, partner, 0).wait_recv()
    stat(r.x_all, r.inv, partner * R, R)
    apply(r.x_all, r.h, r.inv, partner * R, R, 0)
    for o in others:
        owner = 2 * o + 1 - core
        for p in range(pieces):
            lat_copy(owner, p, owner, 0).wait_recv()
        stat(r.x_all, r.inv, owner * R, R)
        apply(r.x_all, r.h, r.inv, owner * R, R, 0)

    scale_k = DK**-0.5

    def rotated(x):
        u, w = x[:, : DK // 2], x[:, DK // 2 :]
        c, s = r.cos_t[...], r.sin_t[...]
        return jnp.concatenate([u * c - w * s, w * c + u * s], axis=1).astype(BF16)

    def st_copy(d, c, to):
        place = rows_of(c * CHUNK, CHUNK)
        return remote(
            r.st_out.at[d, place],
            r.st_in.at[d, place],
            r.st_send.at[d, c],
            r.st_recv.at[d, c],
            {"sp": to},
        )

    loads[10].wait()
    loads[11].wait()
    first = jnp.where(2 * sp < S, 0, 1)
    onward = jnp.where(2 * sp < S, sp + 1, sp - 1)

    def wide(x):
        return jnp.concatenate([x] * (DK // 128), axis=1)

    def head_kv(h, _):
        k = rotated(dot(r.h[...], r.vk[:, cols(h, DK)]) * scale_k)
        r.k[h] = k
        v = dot(r.h[...], r.vv[:, cols(h, DV)]).astype(BF16)
        r.v[:, cols(h, DV)] = v
        kf = k.astype(F32)
        r.loc[first, cols(h, DK), :] = dot_tn((kf * wide(r.ktab[first, h])).astype(BF16), v)

        @pl.when(is_end)
        def _():
            for c in range(per_head):
                place = rows_of(h * DK + c * CHUNK, CHUNK)
                r.st_out[first, place, :] = r.loc[first, place, :].astype(BF16)
                st_copy(first, h * per_head + c, onward).start()

        r.loc[1 - first, cols(h, DK), :] = dot_tn(
            (kf * wide(r.ktab[1 - first, h])).astype(BF16), v
        )
        return 0

    lax.fori_loop(0, nh, head_kv, 0)

    def relay(d, c):
        st_copy(d, c, before[d]).wait_recv()
        place = rows_of(c * CHUNK, CHUNK)
        fade = r.fade[d, lax.div(c, per_head), 0:1, :]
        r.st_out[d, place, :] = (
            r.st_in[d, place, :].astype(F32) * fade + r.loc[d, place, :]
        ).astype(BF16)
        st_copy(d, c, after[d]).start()

    loads[12].wait()
    q_all = dot(r.h[...], r.vq[...])
    for h in range(nh):
        q = rotated(q_all[:, h * DK : (h + 1) * DK])
        r.q[h] = q
        qf = q.astype(F32)
        r.qab[h, :, :DK] = (qf * wide(r.qtab[0, h])).astype(BF16)
        r.qab[h, :, DK:] = (qf * wide(r.qtab[1, h])).astype(BF16)
    loads[13].wait()
    loads[14].wait()

    def gate_item(j):
        pre = dot(r.h[...], r.vg[:, cols(j, TILE)])
        r.g[:, cols(j, TILE)] = pre / (1.0 + jnp.exp(-pre))

    def within_item(h):
        weights = (dot_nt(r.q[h], r.k[h]) * r.mask[h]).astype(BF16)
        r.ret[h] = dot(weights, r.v[:, cols(h, DV)])

    def ctx_forward_item(_):
        for p in sp_peers:
            ctx_copy(p, core, r.ctx_send.at[p], r.ctx_recv.at[0, p], {"sp": p}).wait_recv()
            ctx_copy(p, core, r.ctx_fsend.at[p], r.ctx_recv.at[1, p], {"tp": partner}).start()
        for k, (a, b) in enumerate(opposite):
            m2_copy((a, b), (a, b), k).wait_recv()
        spread(1, r.m2, 0, G)

    def ctx_arrive_item(_):
        for p in sp_peers:
            ctx_copy(
                p, 1 - core, r.ctx_fsend.at[p], r.ctx_recv.at[1, p], {"tp": partner}
            ).wait_recv()

    def ctx_norm_item(j):
        stat(r.c_all, r.cinv, j * 64, 64)
        apply(r.c_all, r.hc, r.cinv, j * 64, 64, 1)

    M = min(CT, TILE)

    def ctx_key_item(j):
        place, h = rows_of(lax.div(j, nh) * M, M), lax.rem(j, nh)
        r.ck[h, place, :] = (dot(r.hc[place, :], r.vk[:, cols(h, DK)]) * scale_k).astype(BF16)

    nv = nh * DV // TILE

    def ctx_value_item(j):
        place, t = rows_of(lax.div(j, nv) * M, M), lax.rem(j, nv)
        r.cv[place, cols(t, TILE)] = dot(r.hc[place, :], r.vv[:, cols(t, TILE)]).astype(BF16)

    def ctx_state_item(j):
        h, d = lax.div(j, 2), lax.rem(j, 2)
        keys = (r.ck[h].astype(F32) * wide(r.ctab[d, h])).astype(BF16)
        away = jnp.where(d == 0, hop[0], hop[1]).astype(F32) * span
        weight = jnp.exp(jnp.full((1, DV), -r.decay[d, h] * away, F32)) * r.gain[h]
        r.base[d, cols(h, DK), :] = dot_tn(keys, r.cv[:, cols(h, DV)]) * weight

    items = [
        (nv, gate_item),
        (1, ctx_forward_item),
        (nh, within_item),
        (1, ctx_arrive_item),
        (CT // 64, ctx_norm_item),
        (CT // M * nh, ctx_key_item),
        (CT // M * nv, ctx_value_item),
        (2 * nh, ctx_state_item),
    ]
    total_items = sum(count for count, _ in items)
    inner = jnp.logical_not(is_end)

    def lap(i, _):
        for d in range(2):
            c = i - PRE - LAG * (hop[d] - 1)

            @pl.when(jnp.logical_and(inner, jnp.logical_and(c >= 0, c < n)))
            def _():
                relay(d, c)

        start = 0
        for count, run in items:

            @pl.when(jnp.logical_and(i >= start, i < start + count))
            def _():
                run(i - start)

            start += count
        return 0

    lax.fori_loop(0, max(PRE + n + LAG * max(S - 3, 0), total_items), lap, 0)

    def project(h, start, count, c):
        return dot(r.gated[h, rows_of(start, count), :], r.vo[h * DV : (h + 1) * DV, cols(c, W)])

    for h in range(nh):
        for d in range(2):

            @pl.when(hop[d] == 0)
            def _():
                r.ent[h, d * DK : (d + 1) * DK, :] = r.base[d, h * DK : (h + 1) * DK, :].astype(
                    BF16
                )

            @pl.when(hop[d] > 0)
            def _():
                def enter(c, _):
                    @pl.when(hop[d] == S - 1)
                    def _():
                        st_copy(d, h * per_head + c, before[d]).wait_recv()

                    place = rows_of(h * DK + c * CHUNK, CHUNK)
                    r.ent[h, rows_of(d * DK + c * CHUNK, CHUNK), :] = (
                        r.st_in[d, place, :].astype(F32) + r.base[d, place, :]
                    ).astype(BF16)
                    return 0

                lax.fori_loop(0, per_head, enter, 0)

        ret = r.ret[h] + dot(r.qab[h], r.ent[h])
        ret = ret - jnp.mean(ret, axis=-1, keepdims=True)
        ret = ret * lax.rsqrt(jnp.mean(ret * ret, axis=-1, keepdims=True) + norm_eps)
        r.gated[h] = (r.g[:, h * DV : (h + 1) * DV] * ret).astype(BF16)
        if h < nh - 1:

            def gather(c, _):
                value = project(h, 0, span, c)
                if h:
                    value = value + r.acc[:, cols(c, W)]
                r.acc[:, cols(c, W)] = value
                return 0

            lax.fori_loop(0, NC, gather, 0)

    def chip_rows(c, o):
        value = project(nh - 1, 2 * o * R, 2 * R, c)
        if nh > 1:
            value = value + r.acc[rows_of(2 * o * R, 2 * R), cols(c, W)]
        value = value.astype(BF16)
        r.part[c, 2 * o] = value[:R]
        r.part[c, 2 * o + 1] = value[R:]

    def p1_copy(c, o):
        return remote(
            r.part.at[c, 2 * o + 1 - core],
            r.p1.at[c, o],
            r.p1_send.at[c, o],
            r.p1_recv.at[c, o],
            {"tp": partner},
        )

    def p2_copy(c):
        return remote(
            r.part.at[c, partner], r.p2.at[c], r.p2_send.at[c], r.p2_recv.at[c], {"tp": partner}
        )

    def x_copy(c, owner, o):
        return remote(
            r.xs.at[c, o],
            r.xr.at[c, owner],
            r.x_send.at[c, o],
            r.x_recv.at[c, owner],
            {"tp": 2 * o + core},
        )

    def away(c, _):
        for o in others:
            chip_rows(c, o)
            p1_copy(c, o).start()
        return 0

    lax.fori_loop(0, NC, away, 0)

    def across(c, _):
        for o in others:
            p1_copy(c, o).wait_recv()
            mine = r.part[c, 2 * o + core].astype(F32)
            r.xs[c, o] = (mine + r.p1[c, o].astype(F32)).astype(BF16)
            x_copy(c, chip, o).start()
        chip_rows(c, chip)
        p2_copy(c).start()
        return 0

    lax.fori_loop(0, NC, across, 0)

    for k in range(len(peers)):
        m1_copy((sp, tp), peers[k], k).wait_send()
        m2_copy((sp, tp), peers[k], k).wait_send()
    for p in range(pieces):
        for o in others:
            lat_copy(tp, p, 2 * o + core, 0).wait_send()
            lat_copy(2 * o + core, p, partner, 1).wait_send()
        lat_copy(tp, p, partner, 0).wait_send()
    for to in sp_peers:
        ctx_out(to).wait_send()
        ctx_copy(to, core, r.ctx_fsend.at[to], r.ctx_recv.at[1, to], {"tp": partner}).wait_send()

    def sent(c, _):
        for d in range(2):

            @pl.when(hop[d] < S - 1)
            def _():
                st_copy(d, c, after[d]).wait_send()

        return 0

    lax.fori_loop(0, n, sent, 0)

    def final(c, _):
        p2_copy(c).wait_recv()
        total = r.part[c, tp].astype(F32) + r.p2[c].astype(F32)
        for o in others:
            x_copy(c, o, o).wait_recv()
            total = total + r.xr[c, o].astype(F32)
        mine = r.x_all[own, cols(c, W)].astype(F32)
        gate = tiled(r.gate[:, cols(c, W)], R // 8)
        out[:, cols(c, W)] = (mine + gate * total).astype(BF16)
        return 0

    lax.fori_loop(0, NC, final, 0)

    def sent_out(c, _):
        for o in others:
            p1_copy(c, o).wait_send()
            x_copy(c, chip, o).wait_send()
        p2_copy(c).wait_send()
        return 0

    lax.fori_loop(0, NC, sent_out, 0)


def body(
    S,
    T,
    latent,
    cond,
    context,
    context_cond,
    norm_gain,
    mod_shift,
    mod_scale,
    mod_gate,
    w_query,
    w_key,
    w_value,
    w_gate,
    w_out,
    decay_rate,
    context_gain,
):
    R, D = latent.shape
    Cr = context.shape[0]
    span, CT = R * T, Cr * S
    nh = w_query.shape[1] // DK
    DV = w_value.shape[1] // nh
    Mr, Mc = mod_shift.shape
    G, GD = Mc // 128, D // 128
    X = T // 2
    W = D // NC
    n = nh * DK // CHUNK
    N = S * T - 1
    pieces = R // PIECE
    v = pltpu.VMEM
    DMA = pltpu.SemaphoreType.DMA
    scratch = dict(
        x_all=v((span, D), BF16),
        c_all=v((CT, D), BF16),
        h=v((span, D), BF16),
        hc=v((CT, D), BF16),
        cond=v((Mr // 128, 128), BF16),
        ccond=v((Mr // 128, 128), BF16),
        ngain=v((GD, 128), BF16),
        decay=pltpu.SMEM(decay_rate.shape, F32),
        gain=pltpu.SMEM(context_gain.shape, F32),
        m_shift=v((Mr, Mc), BF16),
        m_scale=v((Mr, Mc), BF16),
        m_gate=v((Mr, Mc), BF16),
        vq=v(w_query.shape, BF16),
        vk=v(w_key.shape, BF16),
        vv=v(w_value.shape, BF16),
        vg=v(w_gate.shape, BF16),
        vo=v(w_out.shape, BF16),
        m1=v((S, T, 2 * G, 128), F32),
        m2=v((S, T, 3 * G, 128), F32),
        g16=v((3, GD, 128), F32),
        shift=v((2, 8, D), F32),
        mult=v((2, 8, D), F32),
        gate=v((8, D), F32),
        inv=v((span, 128), F32),
        cinv=v((CT, 128), F32),
        cos_t=v((span, DK // 2), F32),
        sin_t=v((span, DK // 2), F32),
        ktab=v((2, nh, span, 128), F32),
        qtab=v((2, nh, span, 128), F32),
        ctab=v((2, nh, CT, 128), F32),
        fade=v((2, nh, 8, DV), F32),
        mask=v((nh, span, span), F32),
        q=v((nh, span, DK), BF16),
        qab=v((nh, span, 2 * DK), BF16),
        k=v((nh, span, DK), BF16),
        v=v((span, nh * DV), BF16),
        ck=v((nh, CT, DK), BF16),
        cv=v((CT, nh * DV), BF16),
        g=v((span, nh * DV), F32),
        ret=v((nh, span, DV), F32),
        gated=v((nh, span, DV), BF16),
        loc=v((2, nh * DK, DV), F32),
        base=v((2, nh * DK, DV), F32),
        st_in=v((2, nh * DK, DV), BF16),
        st_out=v((2, nh * DK, DV), BF16),
        ent=v((nh, 2 * DK, DV), BF16),
        acc=v((span, D), F32),
        part=v((NC, T, R, W), BF16),
        p1=v((NC, X, R, W), BF16),
        p2=v((NC, R, W), BF16),
        xs=v((NC, X, R, W), BF16),
        xr=v((NC, X, R, W), BF16),
        load_sem=DMA((15,)),
        m1_send=DMA((N,)),
        m1_recv=DMA((N,)),
        m2_send=DMA((N,)),
        m2_recv=DMA((N,)),
        lat_send=DMA((2, T, pieces)),
        lat_recv=DMA((T, pieces)),
        ctx_send=DMA((S,)),
        ctx_fsend=DMA((S,)),
        ctx_recv=DMA((2, S)),
        st_send=DMA((2, n)),
        st_recv=DMA((2, n)),
        p1_send=DMA((NC, X)),
        p1_recv=DMA((NC, X)),
        p2_send=DMA((NC,)),
        p2_recv=DMA((NC,)),
        x_send=DMA((NC, X)),
        x_recv=DMA((NC, X)),
    )
    VMEM = pl.BlockSpec(memory_space=pltpu.VMEM)
    ANY = pl.BlockSpec(memory_space=pl.ANY)
    return pl.pallas_call(
        functools.partial(kernel, S, T, tuple(scratch)),
        out_shape=jax.ShapeDtypeStruct((R, D), BF16),
        in_specs=[ANY] * 15,
        out_specs=VMEM,
        scratch_shapes=list(scratch.values()),
        compiler_params=pltpu.CompilerParams(
            collective_id=0, has_side_effects=True, vmem_limit_bytes=60 * 1024 * 1024
        ),
    )(
        latent,
        cond.reshape(Mr // 128, 128),
        context_cond.reshape(Mr // 128, 128),
        context,
        norm_gain.reshape(GD, 128),
        mod_shift,
        mod_scale,
        mod_gate,
        w_query,
        w_key,
        w_value,
        w_gate,
        w_out,
        decay_rate,
        context_gain,
    )


def solution(mesh):
    return jax.shard_map(
        functools.partial(body, mesh.shape["sp"], mesh.shape["tp"]),
        mesh=mesh,
        in_specs=(
            P(("grp", "sp", "tp"), None),
            P(("grp", "sp")),
            P(("grp", "sp"), None),
            P("sp"),
            P(),
            P("sp", "tp"),
            P("sp", "tp"),
            P("sp", "tp"),
            P(None, "tp"),
            P(None, "tp"),
            P(None, "tp"),
            P(None, "tp"),
            P("tp", None),
            P(None, "tp"),
            P("tp"),
        ),
        out_specs=P(("grp", "sp", "tp"), None),
        check_vma=False,
    )
```

time: 68.2 us -> 51.6 us (0.76)
  Pallas kernels: 62.8 us -> 49.7 us
  local copies, waits for them, and re-layouts: 4.4 us -> 1.67 us
  other arithmetic: 0.69 us -> 0 us
    pallas_call x1, Pallas kernels: 62.8 us -> 49.7 us  [body(): pl.pallas_call(functools.partial(kernel, S, T, tuple(scratch)), out_shape...]
    broadcast_in_dim x4 -> x0, local copies, waits for them, and re-layouts: 2.65 us -> none  [the longest x1 1.28 us: body(): norm_gain[None]]
    convert_element_type x1 -> x0, other arithmetic: 0.69 us -> none  [body(): rows = jax.nn.silu(rows).astype(BF16)]
where the time goes in v1:
time: 51.6 us; the launch traced here: 51.4 us
  Pallas kernels  49.7 us (96%)
  local copies, waits for them, and re-layouts  1.67 us (3%)
    pallas_call x1, Pallas kernels, body(): pl.pallas_call(functools.partial(kernel, S, T, tuple(scratch)), out_shape...  49.7 us
    unnamed x1, local copies, waits for them, and re-layouts  1.67 us

profile of v1, /device:TPU:0, one launch (start us, length us, event | category | flops | bytes accessed | tf_op | source)
XLA Modules:
  0.0 51.4 jit_solution(11944041606730265662)
XLA Ops:
  0.0 49.7 %shard_map.145 = bf16[64,2048]{1,0:T(8,128)(2,1)} custom-call(bf16[64,2048]{1,0:T(8,128)(2,1)} %refs_0_.1, bf16[4,128]{1,0:T(4,128)(2,1)} %bitcast.4, bf16[4,128]{1,0:T(4,128)(2,1)} %bitcast.5, bf16[64,2048]{1,0:T(8,128)(2,1)} %refs_3_.1, bf16[16,128]{1,0:T(8,128)(2,1)} %bitcast.3, bf16[512,512]{1,0:T(8,128)(2,1)} %refs_5_.1, bf16[512,512]{1,0:T(8,128)(2,1)} %refs_6_.1, ...), custom_call_target="tpu_custom_call" | custom-call | tf_op jit(solution)/shard_map/pallas_call | solution.py:691
  49.8 1.7 %copy.17 = bf16[64,2048]{1,0:T(8,128)(2,1)} copy(bf16[64,2048]{1,0:T(8,128)(2,1)} %shard_map.145) | data formatting | bytes 524288

commit v2 on v1

--- a/solution.py
+++ b/solution.py
@@ -13,8 +13,10 @@
 GRID_W = 128
 TILE = 256
 PIECE = 16
+EARLY = 1
+OWN = 1
 CHUNK = 32
-LAG = 5
+LAG = (5, 5)
 PRE = 3
 NC = 4
 norm_eps = 1e-06
@@ -47,6 +49,10 @@
 
 def cols(j, size):
     return pl.ds(pl.multiple_of(j * size, size), size)
+
+
+def drain(ref, sem):
+    pltpu.make_async_copy(ref, ref, sem).wait()
 
 
 def tiled(x, count):
@@ -97,6 +103,7 @@
     before = (sp - 1, sp + 1)
     sp_peers = [lax.rem(sp + k, S) for k in range(1, S)]
     others = [lax.rem(chip + k, X) for k in range(1, X)]
+    origins = [lax.rem(chip + X - k, X) for k in range(1, X)]
     peers = [
         (lax.rem(sp + i, S), lax.rem(tp + j, T)) for i in range(S) for j in range(T) if i or j
     ]
@@ -109,11 +116,11 @@
 
     own = rows_of(tp * R, R)
     pairs = [
+        (latent, r.x_all.at[own]),
         (cond, r.cond),
         (context_cond, r.ccond),
         (mod_shift, r.m_shift),
         (mod_scale, r.m_scale),
-        (latent, r.x_all.at[own]),
         (mod_gate, r.m_gate),
         (decay_in, r.decay),
         (gain_in, r.gain),
@@ -131,7 +138,28 @@
     for copy in loads:
         copy.start()
 
-    for copy in loads[:2]:
+    def lat_copy(owner, p, to, sem):
+        place = rows_of(owner * R + p * PIECE, PIECE)
+        return remote(r.x_all.at[place], r.x_all.at[place], r.lat_send.at[0], sem, {"tp": to})
+
+    def lat_whole(owner, to, sem):
+        place = rows_of(owner * R, R)
+        return remote(r.x_all.at[place], r.x_all.at[place], r.lat_send.at[0], sem, {"tp": to})
+
+    def lat_pieces(begin, end):
+        for p in range(begin, end):
+            for k, o in enumerate(others):
+                lat_copy(tp, p, 2 * o + core, r.lat_recv.at[k, p]).start()
+
+    def greet():
+        loads[0].wait()
+        pl.semaphore_wait(barrier, len(peers))
+        lat_pieces(0, EARLY)
+
+    late = 2 * sp >= S
+    pl.when(late)(greet)
+
+    for copy in loads[1:3]:
         copy.wait()
 
     def silu_row(ref):
@@ -142,66 +170,47 @@
     rows = jnp.concatenate(
         [silu_row(r.cond), silu_row(r.ccond), jnp.zeros((14, Mr), F32)], axis=0
     ).astype(BF16)
-    loads[2].wait()
+    loads[3].wait()
     shift_part = dot(rows, r.m_shift[...])
-    loads[3].wait()
+    loads[4].wait()
     scale_part = dot(rows, r.m_scale[...])
+
+    me = sp * T + tp
 
     def lanes(x, row, g):
         return x[row : row + 1, g * 128 : (g + 1) * 128]
 
     for g in range(G):
-        r.m1[sp, tp, g : g + 1, :] = lanes(shift_part, 0, g)
-        r.m1[sp, tp, G + g : G + g + 1, :] = lanes(scale_part, 0, g)
-
-    def m1_copy(owner, to, k):
-        slot = r.m1.at[owner[0], owner[1]]
-        return remote(slot, slot, r.m1_send.at[k], r.m1_recv.at[k], {"sp": to[0], "tp": to[1]})
-
-    def m2_copy(owner, to, k):
-        slot = r.m2.at[owner[0], owner[1]]
-        return remote(slot, slot, r.m2_send.at[k], r.m2_recv.at[k], {"sp": to[0], "tp": to[1]})
-
-    def lat_copy(owner, p, to, which):
-        place = rows_of(owner * R + p * PIECE, PIECE)
+        r.m1[me, g : g + 1, :] = lanes(shift_part, 0, g)
+        r.m1[me, G + g : G + g + 1, :] = lanes(scale_part, 0, g)
+
+    def m_copy(ref, i, to):
         return remote(
-            r.x_all.at[place],
-            r.x_all.at[place],
-            r.lat_send.at[which, to if which == 0 else owner, p],
-            r.lat_recv.at[owner, p],
-            {"tp": to},
+            ref.at[me], ref.at[me], r.m_send.at[i], r.m_recv.at[i], {"sp": to[0], "tp": to[1]}
         )
 
-    def ctx_copy(owner, part_core, send, recv, where):
+    def ctx_copy(owner, part_core, recv, where):
         place = rows_of(owner * Cr + part_core * half, half)
-        return remote(r.c_all.at[place], r.c_all.at[place], send, recv, where)
-
-    def ctx_out(to):
-        return ctx_copy(sp, core, r.ctx_send.at[to], r.ctx_recv.at[0, sp], {"sp": to})
-
-    loads[4].wait()
-    pl.semaphore_wait(barrier, len(peers))
-
-    for k, to in enumerate(peers):
-        m1_copy((sp, tp), to, k).start()
-    for p in range(pieces):
-        for o in others:
-            lat_copy(tp, p, 2 * o + core, 0).start()
-    for p in range(pieces):
-        lat_copy(tp, p, partner, 0).start()
-
-    gate_wait = loads[5]
-    gate_wait.wait()
+        return remote(r.c_all.at[place], r.c_all.at[place], r.ctx_send.at[0], recv, where)
+
+    pl.when(jnp.logical_not(late))(greet)
+
+    for to in peers:
+        m_copy(r.m1, 0, to).start()
+    lat_pieces(EARLY, pieces)
+    lat_whole(tp, partner, r.lat_part.at[0]).start()
+
+    loads[5].wait()
     gate_part = dot(rows, r.m_gate[...])
     for g in range(G):
-        r.m2[sp, tp, g : g + 1, :] = lanes(shift_part, 1, g)
-        r.m2[sp, tp, G + g : G + g + 1, :] = lanes(scale_part, 1, g)
-        r.m2[sp, tp, 2 * G + g : 2 * G + g + 1, :] = lanes(gate_part, 0, g)
+        r.m2[me, g : g + 1, :] = lanes(shift_part, 1, g)
+        r.m2[me, G + g : G + g + 1, :] = lanes(scale_part, 1, g)
+        r.m2[me, 2 * G + g : 2 * G + g + 1, :] = lanes(gate_part, 0, g)
     loads[9].wait()
-    for k, to in enumerate(peers):
-        m2_copy((sp, tp), to, k).start()
+    for to in peers:
+        m_copy(r.m2, 1, to).start()
     for to in sp_peers:
-        ctx_out(to).start()
+        ctx_copy(sp, core, r.ctx_recv.at[0], {"sp": to}).start()
 
     F = DK // 4
     pos = (lax.broadcasted_iota(jnp.int32, (span, 2 * F), 0) + sp * span).astype(F32)
@@ -256,9 +265,9 @@
 
     def spread(row, source, at_shift, at_scale):
         for t in range(T):
-            total = source[0, t]
+            total = source[t]
             for s in range(1, S):
-                total = total + source[s, t]
+                total = total + source[s * T + t]
             r.g16[0, t * G : (t + 1) * G, :] = total[at_shift : at_shift + G]
             r.g16[1, t * G : (t + 1) * G, :] = total[at_scale : at_scale + G]
             if row:
@@ -271,37 +280,21 @@
             if row:
                 r.gate[:, c] = jnp.broadcast_to(r.g16[2, j : j + 1, :], (8, 128))
 
-    stat(r.x_all, r.inv, tp * R, R)
-    for p in range(pieces - 1):
-        for o in others:
-            lat_copy(2 * o + core, p, tp, 0).wait_recv()
-            lat_copy(2 * o + core, p, partner, 1).start()
-    opposite = [(lax.rem(sp - i + S, S), lax.rem(tp - j + T, T)) for i in range(S) for j in range(T) if i or j]
-    for k, (a, b) in enumerate(opposite):
-        m1_copy((a, b), (a, b), k).wait_recv()
-    spread(0, r.m1, 0, G)
-    apply(r.x_all, r.h, r.inv, tp * R, R, 0)
-    for o in others:
-        lat_copy(2 * o + core, pieces - 1, tp, 0).wait_recv()
-        lat_copy(2 * o + core, pieces - 1, partner, 1).start()
-        stat(r.x_all, r.inv, (2 * o + core) * R, R)
-        apply(r.x_all, r.h, r.inv, (2 * o + core) * R, R, 0)
-    for p in range(pieces):
-        lat_copy(partner, p, partner, 0).wait_recv()
-    stat(r.x_all, r.inv, partner * R, R)
-    apply(r.x_all, r.h, r.inv, partner * R, R, 0)
-    for o in others:
-        owner = 2 * o + 1 - core
-        for p in range(pieces):
-            lat_copy(owner, p, owner, 0).wait_recv()
+    def pass_on(p):
+        for k, o in enumerate(origins):
+            owner = 2 * o + core
+            lat_copy(owner, p, tp, r.lat_recv.at[k, p]).wait_recv()
+            lat_copy(owner, p, partner, r.lat_fwd.at[k]).start()
+
+    def rows_done(owner):
         stat(r.x_all, r.inv, owner * R, R)
         apply(r.x_all, r.h, r.inv, owner * R, R, 0)
 
     scale_k = DK**-0.5
 
-    def rotated(x):
+    def rotated(x, place):
         u, w = x[:, : DK // 2], x[:, DK // 2 :]
-        c, s = r.cos_t[...], r.sin_t[...]
+        c, s = r.cos_t[place, :], r.sin_t[place, :]
         return jnp.concatenate([u * c - w * s, w * c + u * s], axis=1).astype(BF16)
 
     def st_copy(d, c, to):
@@ -309,26 +302,36 @@
         return remote(
             r.st_out.at[d, place],
             r.st_in.at[d, place],
-            r.st_send.at[d, c],
+            r.st_send.at[d],
             r.st_recv.at[d, c],
             {"sp": to},
         )
 
-    loads[10].wait()
-    loads[11].wait()
     first = jnp.where(2 * sp < S, 0, 1)
     onward = jnp.where(2 * sp < S, sp + 1, sp - 1)
 
     def wide(x):
         return jnp.concatenate([x] * (DK // 128), axis=1)
 
-    def head_kv(h, _):
-        k = rotated(dot(r.h[...], r.vk[:, cols(h, DK)]) * scale_k)
-        r.k[h] = k
-        v = dot(r.h[...], r.vv[:, cols(h, DV)]).astype(BF16)
-        r.v[:, cols(h, DV)] = v
-        kf = k.astype(F32)
-        r.loc[first, cols(h, DK), :] = dot_tn((kf * wide(r.ktab[first, h])).astype(BF16), v)
+    def key_value(h, o):
+        place = rows_of(2 * o * R, 2 * R)
+        hidden = r.h[place, :]
+        keys = dot(hidden, r.vk[:, cols(h, DK)]) * scale_k
+        r.k[h, place, :] = rotated(keys, place)
+        r.v[place, cols(h, DV)] = dot(hidden, r.vv[:, cols(h, DV)]).astype(BF16)
+
+    def local_state(h, d):
+        keys = (r.k[h].astype(F32) * wide(r.ktab[d, h])).astype(BF16)
+        r.loc[d, cols(h, DK), :] = dot_tn(keys, r.v[:, cols(h, DV)])
+
+    def own_rows(h, _):
+        key_value(h, chip)
+        return 0
+
+    def head_states(h, _):
+        for o in others:
+            key_value(h, o)
+        local_state(h, first)
 
         @pl.when(is_end)
         def _():
@@ -337,12 +340,31 @@
                 r.st_out[first, place, :] = r.loc[first, place, :].astype(BF16)
                 st_copy(first, h * per_head + c, onward).start()
 
-        r.loc[1 - first, cols(h, DK), :] = dot_tn(
-            (kf * wide(r.ktab[1 - first, h])).astype(BF16), v
-        )
+        local_state(h, 1 - first)
         return 0
 
-    lax.fori_loop(0, nh, head_kv, 0)
+    stat(r.x_all, r.inv, tp * R, R)
+    for p in range(pieces - 2):
+        pass_on(p)
+    drain(r.m1.at[pl.ds(0, len(peers))], r.m_recv.at[0])
+    spread(0, r.m1, 0, G)
+    apply(r.x_all, r.h, r.inv, tp * R, R, 0)
+    lat_whole(partner, partner, r.lat_part.at[0]).wait_recv()
+    rows_done(partner)
+    loads[10].wait()
+    loads[11].wait()
+    for p in range(max(pieces - 2, 0), pieces - 1):
+        pass_on(p)
+    lax.fori_loop(0, min(nh, OWN), own_rows, 0)
+    pass_on(pieces - 1)
+    for o in origins:
+        rows_done(2 * o + core)
+    lax.fori_loop(min(nh, OWN), nh, own_rows, 0)
+    for k, o in enumerate(origins):
+        owner = 2 * o + 1 - core
+        lat_whole(owner, owner, r.lat_fwd.at[k]).wait_recv()
+        rows_done(owner)
+    lax.fori_loop(0, nh, head_states, 0)
 
     def relay(d, c):
         st_copy(d, c, before[d]).wait_recv()
@@ -356,7 +378,7 @@
     loads[12].wait()
     q_all = dot(r.h[...], r.vq[...])
     for h in range(nh):
-        q = rotated(q_all[:, h * DK : (h + 1) * DK])
+        q = rotated(q_all[:, h * DK : (h + 1) * DK], slice(0, span))
         r.q[h] = q
         qf = q.astype(F32)
         r.qab[h, :, :DK] = (qf * wide(r.qtab[0, h])).astype(BF16)
@@ -373,18 +395,14 @@
         r.ret[h] = dot(weights, r.v[:, cols(h, DV)])
 
     def ctx_forward_item(_):
+        drain(r.c_all.at[rows_of(0, (S - 1) * half)], r.ctx_recv.at[0])
         for p in sp_peers:
-            ctx_copy(p, core, r.ctx_send.at[p], r.ctx_recv.at[0, p], {"sp": p}).wait_recv()
-            ctx_copy(p, core, r.ctx_fsend.at[p], r.ctx_recv.at[1, p], {"tp": partner}).start()
-        for k, (a, b) in enumerate(opposite):
-            m2_copy((a, b), (a, b), k).wait_recv()
+            ctx_copy(p, core, r.ctx_recv.at[1], {"tp": partner}).start()
+        drain(r.m2.at[pl.ds(0, len(peers))], r.m_recv.at[1])
         spread(1, r.m2, 0, G)
 
     def ctx_arrive_item(_):
-        for p in sp_peers:
-            ctx_copy(
-                p, 1 - core, r.ctx_fsend.at[p], r.ctx_recv.at[1, p], {"tp": partner}
-            ).wait_recv()
+        drain(r.c_all.at[rows_of(0, (S - 1) * half)], r.ctx_recv.at[1])
 
     def ctx_norm_item(j):
         stat(r.c_all, r.cinv, j * 64, 64)
@@ -423,8 +441,8 @@
     inner = jnp.logical_not(is_end)
 
     def lap(i, _):
-        for d in range(2):
-            c = i - PRE - LAG * (hop[d] - 1)
+        for d in (1, 0):
+            c = i - PRE - LAG[d] * (hop[d] - 1)
 
             @pl.when(jnp.logical_and(inner, jnp.logical_and(c >= 0, c < n)))
             def _():
@@ -440,7 +458,7 @@
             start += count
         return 0
 
-    lax.fori_loop(0, max(PRE + n + LAG * max(S - 3, 0), total_items), lap, 0)
+    lax.fori_loop(0, max(PRE + n + max(LAG) * max(S - 3, 0), total_items), lap, 0)
 
     def project(h, start, count, c):
         return dot(r.gated[h, rows_of(start, count), :], r.vo[h * DV : (h + 1) * DV, cols(c, W)])
@@ -492,93 +510,73 @@
         r.part[c, 2 * o] = value[:R]
         r.part[c, 2 * o + 1] = value[R:]
 
-    def p1_copy(c, o):
+    def p1_copy(c, k, o):
         return remote(
             r.part.at[c, 2 * o + 1 - core],
-            r.p1.at[c, o],
-            r.p1_send.at[c, o],
-            r.p1_recv.at[c, o],
+            r.p1.at[c, k],
+            r.out_send.at[0],
+            r.p1_recv.at[c, k],
             {"tp": partner},
         )
 
     def p2_copy(c):
         return remote(
-            r.part.at[c, partner], r.p2.at[c], r.p2_send.at[c], r.p2_recv.at[c], {"tp": partner}
+            r.part.at[c, partner], r.p2.at[c], r.out_send.at[0], r.p2_recv.at[0], {"tp": partner}
         )
 
-    def x_copy(c, owner, o):
+    def x_copy(c, k, o):
         return remote(
-            r.xs.at[c, o],
-            r.xr.at[c, owner],
-            r.x_send.at[c, o],
-            r.x_recv.at[c, owner],
+            r.xs.at[c, k],
+            r.xr.at[c, k],
+            r.out_send.at[0],
+            r.x_recv.at[c, k],
             {"tp": 2 * o + core},
         )
 
     def away(c, _):
-        for o in others:
+        for k, o in enumerate(others):
             chip_rows(c, o)
-            p1_copy(c, o).start()
+            p1_copy(c, k, o).start()
         return 0
 
     lax.fori_loop(0, NC, away, 0)
 
     def across(c, _):
-        for o in others:
-            p1_copy(c, o).wait_recv()
+        for k, o in enumerate(others):
+            p1_copy(c, k, o).wait_recv()
             mine = r.part[c, 2 * o + core].astype(F32)
-            r.xs[c, o] = (mine + r.p1[c, o].astype(F32)).astype(BF16)
-            x_copy(c, chip, o).start()
+            r.xs[c, k] = (mine + r.p1[c, k].astype(F32)).astype(BF16)
+            x_copy(c, k, o).start()
         chip_rows(c, chip)
         p2_copy(c).start()
         return 0
 
     lax.fori_loop(0, NC, across, 0)
 
-    for k in range(len(peers)):
-        m1_copy((sp, tp), peers[k], k).wait_send()
-        m2_copy((sp, tp), peers[k], k).wait_send()
-    for p in range(pieces):
-        for o in others:
-            lat_copy(tp, p, 2 * o + core, 0).wait_send()
-            lat_copy(2 * o + core, p, partner, 1).wait_send()
-        lat_copy(tp, p, partner, 0).wait_send()
-    for to in sp_peers:
-        ctx_out(to).wait_send()
-        ctx_copy(to, core, r.ctx_fsend.at[to], r.ctx_recv.at[1, to], {"tp": partner}).wait_send()
-
-    def sent(c, _):
-        for d in range(2):
-
-            @pl.when(hop[d] < S - 1)
-            def _():
-                st_copy(d, c, after[d]).wait_send()
-
-        return 0
-
-    lax.fori_loop(0, n, sent, 0)
+    drain(r.m1.at[pl.ds(0, len(peers))], r.m_send.at[0])
+    drain(r.m2.at[pl.ds(0, len(peers))], r.m_send.at[1])
+    drain(r.x_all.at[rows_of(0, (T - 1) * R)], r.lat_send.at[0])
+    drain(r.c_all.at[rows_of(0, (S - 1) * Cr)], r.ctx_send.at[0])
+    for d in range(2):
+
+        @pl.when(hop[d] < S - 1)
+        def _():
+            drain(r.st_out.at[d], r.st_send.at[d])
+
+    drain(r.p2, r.p2_recv.at[0])
 
     def final(c, _):
-        p2_copy(c).wait_recv()
         total = r.part[c, tp].astype(F32) + r.p2[c].astype(F32)
-        for o in others:
-            x_copy(c, o, o).wait_recv()
-            total = total + r.xr[c, o].astype(F32)
+        for k, o in enumerate(origins):
+            x_copy(c, k, o).wait_recv()
+            total = total + r.xr[c, k].astype(F32)
         mine = r.x_all[own, cols(c, W)].astype(F32)
         gate = tiled(r.gate[:, cols(c, W)], R // 8)
         out[:, cols(c, W)] = (mine + gate * total).astype(BF16)
         return 0
 
     lax.fori_loop(0, NC, final, 0)
-
-    def sent_out(c, _):
-        for o in others:
-            p1_copy(c, o).wait_send()
-            x_copy(c, chip, o).wait_send()
-        p2_copy(c).wait_send()
-        return 0
-
-    lax.fori_loop(0, NC, sent_out, 0)
+    drain(r.part.at[:, pl.ds(0, T - 1)], r.out_send.at[0])
 
 
 def body(
@@ -610,7 +608,6 @@
     X = T // 2
     W = D // NC
     n = nh * DK // CHUNK
-    N = S * T - 1
     pieces = R // PIECE
     v = pltpu.VMEM
     DMA = pltpu.SemaphoreType.DMA
@@ -632,8 +629,8 @@
         vv=v(w_value.shape, BF16),
         vg=v(w_gate.shape, BF16),
         vo=v(w_out.shape, BF16),
-        m1=v((S, T, 2 * G, 128), F32),
-        m2=v((S, T, 3 * G, 128), F32),
+        m1=v((S * T, 2 * G, 128), F32),
+        m2=v((S * T, 3 * G, 128), F32),
         g16=v((3, GD, 128), F32),
         shift=v((2, 8, D), F32),
         mult=v((2, 8, D), F32),
@@ -663,34 +660,31 @@
         ent=v((nh, 2 * DK, DV), BF16),
         acc=v((span, D), F32),
         part=v((NC, T, R, W), BF16),
-        p1=v((NC, X, R, W), BF16),
+        p1=v((NC, X - 1, R, W), BF16),
         p2=v((NC, R, W), BF16),
-        xs=v((NC, X, R, W), BF16),
-        xr=v((NC, X, R, W), BF16),
+        xs=v((NC, X - 1, R, W), BF16),
+        xr=v((NC, X - 1, R, W), BF16),
         load_sem=DMA((15,)),
-        m1_send=DMA((N,)),
-        m1_recv=DMA((N,)),
-        m2_send=DMA((N,)),
-        m2_recv=DMA((N,)),
-        lat_send=DMA((2, T, pieces)),
-        lat_recv=DMA((T, pieces)),
-        ctx_send=DMA((S,)),
-        ctx_fsend=DMA((S,)),
-        ctx_recv=DMA((2, S)),
-        st_send=DMA((2, n)),
+        m_send=DMA((2,)),
+        m_recv=DMA((2,)),
+        lat_send=DMA((1,)),
+        lat_recv=DMA((X - 1, pieces)),
+        lat_part=DMA((1,)),
+        lat_fwd=DMA((X - 1,)),
+        ctx_send=DMA((1,)),
+        ctx_recv=DMA((2,)),
+        st_send=DMA((2,)),
         st_recv=DMA((2, n)),
-        p1_send=DMA((NC, X)),
-        p1_recv=DMA((NC, X)),
-        p2_send=DMA((NC,)),
-        p2_recv=DMA((NC,)),
-        x_send=DMA((NC, X)),
-        x_recv=DMA((NC, X)),
+        out_send=DMA((1,)),
+        p1_recv=DMA((NC, X - 1)),
+        p2_recv=DMA((1,)),
+        x_recv=DMA((NC, X - 1)),
     )
     VMEM = pl.BlockSpec(memory_space=pltpu.VMEM)
     ANY = pl.BlockSpec(memory_space=pl.ANY)
     return pl.pallas_call(
         functools.partial(kernel, S, T, tuple(scratch)),
-        out_shape=jax.ShapeDtypeStruct((R, D), BF16),
+        out_shape=pltpu.VMEM((R, D), BF16),
         in_specs=[ANY] * 15,
         out_specs=VMEM,
         scratch_shapes=list(scratch.values()),

time: 51.6 us -> 47.9 us (0.928)
  Pallas kernels: 49.7 us -> 47.1 us
  local copies, waits for them, and re-layouts: 1.67 us -> 0.71 us
    pallas_call x1, Pallas kernels: 49.7 us -> 47.1 us  [body(): pl.pallas_call(functools.partial(kernel, S, T, tuple(scratch)), out_shape...]
    unnamed x1, local copies, waits for them, and re-layouts: 1.67 us -> 0.71 us
where the time goes in v2:
time: 47.9 us; the launch traced here: 47.8 us
  Pallas kernels  47.1 us (98%)
  local copies, waits for them, and re-layouts  0.71 us (1%)
    pallas_call x1, Pallas kernels, body(): pl.pallas_call(functools.partial(kernel, S, T, tuple(scratch)), out_shape...  47.1 us

profile of v2, /device:TPU:0, one launch (start us, length us, event | category | flops | bytes accessed | tf_op | source)
XLA Modules:
  0.0 47.8 jit_solution(5698042935185093875)
XLA Ops:
  0.0 47.1 %shard_map.145 = bf16[64,2048]{1,0:T(8,128)(2,1)S(1)} custom-call(bf16[64,2048]{1,0:T(8,128)(2,1)} %refs_0_.1, bf16[4,128]{1,0:T(4,128)(2,1)} %bitcast.4, bf16[4,128]{1,0:T(4,128)(2,1)} %bitcast.5, bf16[64,2048]{1,0:T(8,128)(2,1)} %refs_3_.1, bf16[16,128]{1,0:T(8,128)(2,1)} %bitcast.3, bf16[512,512]{1,0:T(8,128)(2,1)} %refs_5_.1, bf16[512,512]{1,0:T(8,128)(2,1)} %refs_6_.1, ...), custom_call_target="tpu_custom_call" | custom-call | tf_op jit(solution)/shard_map/pallas_call | solution.py:685
  47.1 0.7 %copy.17 = bf16[64,2048]{1,0:T(8,128)(2,1)} copy(bf16[64,2048]{1,0:T(8,128)(2,1)S(1)} %shard_map.145) | data formatting | bytes 524288

commit v3 on v2

--- a/solution.py
+++ b/solution.py
@@ -16,9 +16,10 @@
 EARLY = 1
 OWN = 1
 CHUNK = 32
-LAG = (5, 5)
-PRE = 3
-NC = 4
+LAG = (6, 4)
+PRE = 1
+SPARE = (1, 1)
+NC = 2
 norm_eps = 1e-06
 rope_base = 10000.0
 MESH = pl.DeviceIdType.MESH
@@ -429,8 +430,10 @@
 
     items = [
         (nv, gate_item),
+        (nh, within_item),
+        (SPARE[0], None),
         (1, ctx_forward_item),
-        (nh, within_item),
+        (SPARE[1], None),
         (1, ctx_arrive_item),
         (CT // 64, ctx_norm_item),
         (CT // M * nh, ctx_key_item),
@@ -450,10 +453,11 @@
 
         start = 0
         for count, run in items:
-
-            @pl.when(jnp.logical_and(i >= start, i < start + count))
-            def _():
-                run(i - start)
+            if run is not None:
+
+                @pl.when(jnp.logical_and(i >= start, i < start + count))
+                def _():
+                    run(i - start)
 
             start += count
         return 0

time: 47.9 us -> 46.7 us (0.975)
  Pallas kernels: 47.1 us -> 45.9 us
    pallas_call x1, Pallas kernels: 47.1 us -> 45.9 us  [body(): pl.pallas_call(functools.partial(kernel, S, T, tuple(scratch)), out_shape...]
where the time goes in v3:
time: 46.7 us; the launch traced here: 46.6 us
  Pallas kernels  45.9 us (98%)
  local copies, waits for them, and re-layouts  0.71 us (2%)
    pallas_call x1, Pallas kernels, body(): pl.pallas_call(functools.partial(kernel, S, T, tuple(scratch)), out_shape...  45.9 us

profile of v3, /device:TPU:0, one launch (start us, length us, event | category | flops | bytes accessed | tf_op | source)
XLA Modules:
  0.0 46.6 jit_solution(215093124336261627)
XLA Ops:
  0.0 45.9 %shard_map.145 = bf16[64,2048]{1,0:T(8,128)(2,1)S(1)} custom-call(bf16[64,2048]{1,0:T(8,128)(2,1)} %refs_0_.1, bf16[4,128]{1,0:T(4,128)(2,1)} %bitcast.4, bf16[4,128]{1,0:T(4,128)(2,1)} %bitcast.5, bf16[64,2048]{1,0:T(8,128)(2,1)} %refs_3_.1, bf16[16,128]{1,0:T(8,128)(2,1)} %bitcast.3, bf16[512,512]{1,0:T(8,128)(2,1)} %refs_5_.1, bf16[512,512]{1,0:T(8,128)(2,1)} %refs_6_.1, ...), custom_call_target="tpu_custom_call" | custom-call | tf_op jit(solution)/shard_map/pallas_call | solution.py:689
  45.9 0.7 %copy.17 = bf16[64,2048]{1,0:T(8,128)(2,1)} copy(bf16[64,2048]{1,0:T(8,128)(2,1)S(1)} %shard_map.145) | data formatting | bytes 524288

commit v4 on v3

--- a/solution.py
+++ b/solution.py
@@ -18,8 +18,9 @@
 CHUNK = 32
 LAG = (6, 4)
 PRE = 1
-SPARE = (1, 1)
+SPARE = (1, 1, 1, 2)
 NC = 2
+DIRECT = 256
 norm_eps = 1e-06
 rope_base = 10000.0
 MESH = pl.DeviceIdType.MESH
@@ -96,7 +97,7 @@
     chip, core = tp // 2, lax.rem(tp, 2)
     partner = tp + 1 - 2 * core
     is_end = jnp.logical_or(sp == 0, sp == S - 1)
-    W = D // NC
+    V = (D - DIRECT) // NC
     per_head = DK // CHUNK
     n = nh * per_head
     hop = (sp, S - 1 - sp)
@@ -185,10 +186,18 @@
         r.m1[me, g : g + 1, :] = lanes(shift_part, 0, g)
         r.m1[me, G + g : G + g + 1, :] = lanes(scale_part, 0, g)
 
-    def m_copy(ref, i, to):
+    def m_copy(ref, i, to, slot=me):
         return remote(
-            ref.at[me], ref.at[me], r.m_send.at[i], r.m_recv.at[i], {"sp": to[0], "tp": to[1]}
+            ref.at[slot],
+            ref.at[slot],
+            r.m_send.at[i],
+            r.m_recv.at[i],
+            {"sp": to[0], "tp": to[1]},
         )
+
+    sp_all = [sp] + sp_peers
+    near = [(a, b) for a in sp_all for b in (tp, partner) if a is not sp or b is not tp]
+    across_x = [(a, 2 * o + core) for a in sp_all for o in others]
 
     def ctx_copy(owner, part_core, recv, where):
         place = rows_of(owner * Cr + part_core * half, half)
@@ -196,7 +205,9 @@
 
     pl.when(jnp.logical_not(late))(greet)
 
-    for to in peers:
+    for to in across_x:
+        m_copy(r.m1, 2, to).start()
+    for to in near:
         m_copy(r.m1, 0, to).start()
     lat_pieces(EARLY, pieces)
     lat_whole(tp, partner, r.lat_part.at[0]).start()
@@ -347,7 +358,12 @@
     stat(r.x_all, r.inv, tp * R, R)
     for p in range(pieces - 2):
         pass_on(p)
-    drain(r.m1.at[pl.ds(0, len(peers))], r.m_recv.at[0])
+    drain(r.m1.at[pl.ds(0, len(across_x))], r.m_recv.at[2])
+    for a in sp_all:
+        for o in origins:
+            m_copy(r.m1, 3, (sp, partner), a * T + 2 * o + core).start()
+    drain(r.m1.at[pl.ds(0, len(near))], r.m_recv.at[0])
+    drain(r.m1.at[pl.ds(0, len(across_x))], r.m_recv.at[3])
     spread(0, r.m1, 0, G)
     apply(r.x_all, r.h, r.inv, tp * R, R, 0)
     lat_whole(partner, partner, r.lat_part.at[0]).wait_recv()
@@ -437,7 +453,9 @@
         (1, ctx_arrive_item),
         (CT // 64, ctx_norm_item),
         (CT // M * nh, ctx_key_item),
+        (SPARE[2], None),
         (CT // M * nv, ctx_value_item),
+        (SPARE[3], None),
         (2 * nh, ctx_state_item),
     ]
     total_items = sum(count for count, _ in items)
@@ -464,8 +482,8 @@
 
     lax.fori_loop(0, max(PRE + n + max(LAG) * max(S - 3, 0), total_items), lap, 0)
 
-    def project(h, start, count, c):
-        return dot(r.gated[h, rows_of(start, count), :], r.vo[h * DV : (h + 1) * DV, cols(c, W)])
+    def project(h, start, count, place):
+        return dot(r.gated[h, rows_of(start, count), :], r.vo[h * DV : (h + 1) * DV, place])
 
     for h in range(nh):
         for d in range(2):
@@ -498,66 +516,82 @@
         if h < nh - 1:
 
             def gather(c, _):
-                value = project(h, 0, span, c)
+                place = cols(c, D // 4)
+                value = project(h, 0, span, place)
                 if h:
-                    value = value + r.acc[:, cols(c, W)]
-                r.acc[:, cols(c, W)] = value
+                    value = value + r.acc[:, place]
+                r.acc[:, place] = value
                 return 0
 
-            lax.fori_loop(0, NC, gather, 0)
-
-    def chip_rows(c, o):
-        value = project(nh - 1, 2 * o * R, 2 * R, c)
+            lax.fori_loop(0, 4, gather, 0)
+
+    def chip_rows(dst, o, place):
+        value = project(nh - 1, 2 * o * R, 2 * R, place)
         if nh > 1:
-            value = value + r.acc[rows_of(2 * o * R, 2 * R), cols(c, W)]
+            value = value + r.acc[rows_of(2 * o * R, 2 * R), place]
         value = value.astype(BF16)
-        r.part[c, 2 * o] = value[:R]
-        r.part[c, 2 * o + 1] = value[R:]
-
-    def p1_copy(c, k, o):
+        dst[0] = value[:R]
+        dst[1] = value[R:]
+
+    strips = [slice(DIRECT + c * V, DIRECT + (c + 1) * V) for c in range(NC)]
+
+    def d_copy(k, o, c):
         return remote(
-            r.part.at[c, 2 * o + 1 - core],
+            r.dpart.at[k, c],
+            r.dr.at[k, core],
+            r.out_send.at[0],
+            r.d_recv.at[0],
+            {"tp": 2 * o + c},
+        )
+
+    def p1_copy(c, k):
+        return remote(
+            r.part.at[c, k, 1 - core],
             r.p1.at[c, k],
-            r.out_send.at[0],
+            r.out_send.at[1],
             r.p1_recv.at[c, k],
             {"tp": partner},
-        )
-
-    def p2_copy(c):
-        return remote(
-            r.part.at[c, partner], r.p2.at[c], r.out_send.at[0], r.p2_recv.at[0], {"tp": partner}
         )
 
     def x_copy(c, k, o):
         return remote(
             r.xs.at[c, k],
             r.xr.at[c, k],
-            r.out_send.at[0],
+            r.out_send.at[2],
             r.x_recv.at[c, k],
             {"tp": 2 * o + core},
         )
 
-    def away(c, _):
+    def p2_copy(place):
+        return remote(
+            r.home.at[1 - core, :, place],
+            r.p2.at[:, place],
+            r.out_send.at[3],
+            r.p2_recv.at[0],
+            {"tp": partner},
+        )
+
+    for k, o in enumerate(others):
+        chip_rows(r.dpart.at[k], o, slice(0, DIRECT))
+        for c in range(2):
+            d_copy(k, o, c).start()
+    for c in range(NC):
         for k, o in enumerate(others):
-            chip_rows(c, o)
-            p1_copy(c, k, o).start()
-        return 0
-
-    lax.fori_loop(0, NC, away, 0)
-
-    def across(c, _):
+            chip_rows(r.part.at[c, k], o, strips[c])
+            p1_copy(c, k).start()
+    for c in range(NC):
         for k, o in enumerate(others):
-            p1_copy(c, k, o).wait_recv()
-            mine = r.part[c, 2 * o + core].astype(F32)
+            p1_copy(c, k).wait_recv()
+            mine = r.part[c, k, core].astype(F32)
             r.xs[c, k] = (mine + r.p1[c, k].astype(F32)).astype(BF16)
             x_copy(c, k, o).start()
-        chip_rows(c, chip)
-        p2_copy(c).start()
-        return 0
-
-    lax.fori_loop(0, NC, across, 0)
-
-    drain(r.m1.at[pl.ds(0, len(peers))], r.m_send.at[0])
+        place = slice(c * (D // NC), (c + 1) * (D // NC))
+        chip_rows(r.home.at[:, :, place], chip, slice(place.start, place.stop))
+        p2_copy(place).start()
+
+    drain(r.m1.at[pl.ds(0, len(near))], r.m_send.at[0])
+    drain(r.m1.at[pl.ds(0, len(across_x))], r.m_send.at[2])
+    drain(r.m1.at[pl.ds(0, len(across_x))], r.m_send.at[3])
     drain(r.m2.at[pl.ds(0, len(peers))], r.m_send.at[1])
     drain(r.x_all.at[rows_of(0, (T - 1) * R)], r.lat_send.at[0])
     drain(r.c_all.at[rows_of(0, (S - 1) * Cr)], r.ctx_send.at[0])
@@ -569,18 +603,23 @@
 
     drain(r.p2, r.p2_recv.at[0])
 
-    def final(c, _):
-        total = r.part[c, tp].astype(F32) + r.p2[c].astype(F32)
+    def final(place, arrived):
+        total = r.home[core, :, place].astype(F32) + r.p2[:, place].astype(F32)
+        for piece in arrived:
+            total = total + piece.astype(F32)
+        mine = r.x_all[own, place].astype(F32)
+        out[:, place] = (mine + tiled(r.gate[:, place], R // 8) * total).astype(BF16)
+
+    drain(r.dr, r.d_recv.at[0])
+    final(slice(0, DIRECT), [r.dr[k, c] for k in range(X - 1) for c in range(2)])
+    for c in range(NC):
         for k, o in enumerate(origins):
             x_copy(c, k, o).wait_recv()
-            total = total + r.xr[c, k].astype(F32)
-        mine = r.x_all[own, cols(c, W)].astype(F32)
-        gate = tiled(r.gate[:, cols(c, W)], R // 8)
-        out[:, cols(c, W)] = (mine + gate * total).astype(BF16)
-        return 0
-
-    lax.fori_loop(0, NC, final, 0)
-    drain(r.part.at[:, pl.ds(0, T - 1)], r.out_send.at[0])
+        final(strips[c], [r.xr[c, k] for k in range(X - 1)])
+    drain(r.dpart, r.out_send.at[0])
+    drain(r.p1, r.out_send.at[1])
+    drain(r.xs, r.out_send.at[2])
+    drain(r.p2, r.out_send.at[3])
 
 
 def body(
@@ -610,7 +649,7 @@
     Mr, Mc = mod_shift.shape
     G, GD = Mc // 128, D // 128
     X = T // 2
-    W = D // NC
+    V = (D - DIRECT) // NC
     n = nh * DK // CHUNK
     pieces = R // PIECE
     v = pltpu.VMEM
@@ -663,14 +702,17 @@
         st_out=v((2, nh * DK, DV), BF16),
         ent=v((nh, 2 * DK, DV), BF16),
         acc=v((span, D), F32),
-        part=v((NC, T, R, W), BF16),
-        p1=v((NC, X - 1, R, W), BF16),
-        p2=v((NC, R, W), BF16),
-        xs=v((NC, X - 1, R, W), BF16),
-        xr=v((NC, X - 1, R, W), BF16),
+        dpart=v((X - 1, 2, R, DIRECT), BF16),
+        dr=v((X - 1, 2, R, DIRECT), BF16),
+        part=v((NC, X - 1, 2, R, V), BF16),
+        p1=v((NC, X - 1, R, V), BF16),
+        xs=v((NC, X - 1, R, V), BF16),
+        xr=v((NC, X - 1, R, V), BF16),
+        home=v((2, R, D), BF16),
+        p2=v((R, D), BF16),
         load_sem=DMA((15,)),
-        m_send=DMA((2,)),
-        m_recv=DMA((2,)),
+        m_send=DMA((4,)),
+        m_recv=DMA((4,)),
         lat_send=DMA((1,)),
         lat_recv=DMA((X - 1, pieces)),
         lat_part=DMA((1,)),
@@ -679,7 +721,8 @@
         ctx_recv=DMA((2,)),
         st_send=DMA((2,)),
         st_recv=DMA((2, n)),
-        out_send=DMA((1,)),
+        out_send=DMA((4,)),
+        d_recv=DMA((1,)),
         p1_recv=DMA((NC, X - 1)),
         p2_recv=DMA((1,)),
         x_recv=DMA((NC, X - 1)),

time: 46.7 us -> 45.9 us (0.983)
  Pallas kernels: 45.9 us -> 45.1 us
    pallas_call x1, Pallas kernels: 45.9 us -> 45.1 us  [body(): pl.pallas_call(functools.partial(kernel, S, T, tuple(scratch)), out_shape...]
where the time goes in v4:
time: 45.9 us; the launch traced here: 45.8 us
  Pallas kernels  45.1 us (98%)
  local copies, waits for them, and re-layouts  0.71 us (2%)
    pallas_call x1, Pallas kernels, body(): pl.pallas_call(functools.partial(kernel, S, T, tuple(scratch)), out_shape...  45.1 us

profile of v4, /device:TPU:0, one launch (start us, length us, event | category | flops | bytes accessed | tf_op | source)
XLA Modules:
  0.0 45.8 jit_solution(18375103176968372771)
XLA Ops:
  0.0 45.1 %shard_map.145 = bf16[64,2048]{1,0:T(8,128)(2,1)S(1)} custom-call(bf16[64,2048]{1,0:T(8,128)(2,1)} %refs_0_.1, bf16[4,128]{1,0:T(4,128)(2,1)} %bitcast.4, bf16[4,128]{1,0:T(4,128)(2,1)} %bitcast.5, bf16[64,2048]{1,0:T(8,128)(2,1)} %refs_3_.1, bf16[16,128]{1,0:T(8,128)(2,1)} %bitcast.3, bf16[512,512]{1,0:T(8,128)(2,1)} %refs_5_.1, bf16[512,512]{1,0:T(8,128)(2,1)} %refs_6_.1, ...), custom_call_target="tpu_custom_call" | custom-call | tf_op jit(solution)/shard_map/pallas_call | solution.py:732
  45.1 0.7 %copy.17 = bf16[64,2048]{1,0:T(8,128)(2,1)} copy(bf16[64,2048]{1,0:T(8,128)(2,1)S(1)} %shard_map.145) | data formatting | bytes 524288

commit v5 on v4

--- a/solution.py
+++ b/solution.py
@@ -509,7 +509,10 @@
 
                 lax.fori_loop(0, per_head, enter, 0)
 
-        ret = r.ret[h] + dot(r.qab[h], r.ent[h])
+            if d == 0:
+                r.ret[h] = r.ret[h] + dot(r.qab[h, :, :DK], r.ent[h, :DK])
+
+        ret = r.ret[h] + dot(r.qab[h, :, DK:], r.ent[h, DK:])
         ret = ret - jnp.mean(ret, axis=-1, keepdims=True)
         ret = ret * lax.rsqrt(jnp.mean(ret * ret, axis=-1, keepdims=True) + norm_eps)
         r.gated[h] = (r.g[:, h * DV : (h + 1) * DV] * ret).astype(BF16)

time: 45.9 us -> 46 us (level)
  no operation moved by 1% of the time
where the time goes in v5:
time: 46 us; the launch traced here: 45.7 us
  Pallas kernels  45 us (98%)
  local copies, waits for them, and re-layouts  0.71 us (2%)
    pallas_call x1, Pallas kernels, body(): pl.pallas_call(functools.partial(kernel, S, T, tuple(scratch)), out_shape...  45 us

profile of v5, /device:TPU:0, one launch (start us, length us, event | category | flops | bytes accessed | tf_op | source)
XLA Modules:
  0.0 45.7 jit_solution(3029382554620825034)
XLA Ops:
  0.0 45.0 %shard_map.145 = bf16[64,2048]{1,0:T(8,128)(2,1)S(1)} custom-call(bf16[64,2048]{1,0:T(8,128)(2,1)} %refs_0_.1, bf16[4,128]{1,0:T(4,128)(2,1)} %bitcast.4, bf16[4,128]{1,0:T(4,128)(2,1)} %bitcast.5, bf16[64,2048]{1,0:T(8,128)(2,1)} %refs_3_.1, bf16[16,128]{1,0:T(8,128)(2,1)} %bitcast.3, bf16[512,512]{1,0:T(8,128)(2,1)} %refs_5_.1, bf16[512,512]{1,0:T(8,128)(2,1)} %refs_6_.1, ...), custom_call_target="tpu_custom_call" | custom-call | tf_op jit(solution)/shard_map/pallas_call | solution.py:735
  45.0 0.7 %copy.17 = bf16[64,2048]{1,0:T(8,128)(2,1)} copy(bf16[64,2048]{1,0:T(8,128)(2,1)S(1)} %shard_map.145) | data formatting | bytes 524288
